TPU v7x, 128 devices: a whole 4x4x4 slice. The times are simulated.
128 devices in a mesh: fs: 16 (over z, y), tp: 8 (over x, core).
Axes of the slice: x: 4, y: 4, z: 4, core: 2. Of those that a mesh axis runs over, the one named last changes fastest.
Arguments:
- resid: bfloat16 [24576, 2048], P(('fs', 'tp')), may hold values from -6 to 6
- norm1_gain: float32 [2048], replicated, may hold values from 0.1 to 1.9
- w_value: float32 [2048, 2048], P('fs', 'tp'), may hold values from -0.125 to 0.125
- w_gate: float32 [2048, 2048], P('fs', 'tp'), may hold values from -0.125 to 0.125
- value_scale: float32 [2048], replicated, may hold values from 0.3 to 3
- gate_scale: float32 [2048], replicated, may hold values from 0.5 to 3
- conv_taps: float32 [31, 2048], replicated, may hold values from -1 to 1
- conv_gain: float32 [2048], replicated, may hold values from 0.1 to 1.9
- w_point: float32 [2048, 2048], P('tp', 'fs'), may hold values from -0.125 to 0.125
- point_scale: float32 [2048], P('fs'), may hold values from 0.5 to 3
- norm2_gain: float32 [2048], replicated, may hold values from 0.1 to 1.9
- w_up: float32 [2048, 8192], P('fs', 'tp'), may hold values from -0.125 to 0.125
- up_scale: float32 [8192], P('tp'), may hold values from 0.5 to 1.5
- w_down: float32 [8192, 2048], P('tp', 'fs'), may hold values from -0.0625 to 0.0625
- down_scale: float32 [2048], P('fs'), may hold values from 0.3 to 1
Outputs:
- layer_out: bfloat16 [24576, 2048], P(('fs', 'tp'))
All inputs are finite; a program needn't handle non-finite values.
Results may differ from a plain program's by a relative error of at most 0.015.
Values may be sent and summed in bfloat16 or wider, within the bound.
A program may use at most 128 MiB of HBM per device.

v0:
```python
import jax
import jax.numpy as jnp
from jax import lax
from jax.sharding import PartitionSpec as P

GROUPS = 4


def gather_turned(arrays, axis, dims):
    turned = [jnp.moveaxis(a, dim, 0) for a, dim in zip(arrays, dims)]
    both = jnp.concatenate([t.reshape(len(t), -1) for t in turned], axis=1)
    result, at, done = (lax.all_gather(both, axis, axis=0, tiled=True), 0, [])
    for t, dim in zip(turned, dims):
        slab = result[:, at : at + t[0].size].reshape(-1, *t.shape[1:])
        done.append(jnp.moveaxis(slab, 0, dim))
        at += t[0].size
    return tuple(done)


def laid_out(pieces, dim):
    shape = list(pieces.shape[1:])
    shape[dim] *= pieces.shape[0]
    return jnp.moveaxis(pieces, 0, dim).reshape(shape)


def from_everyone(x, axis):
    copies = jnp.broadcast_to(x, (lax.axis_size(axis), *x.shape))
    return lax.all_to_all(copies, axis, split_axis=0, concat_axis=0, tiled=True)


def gather_directly(x, axis, dim):
    return laid_out(from_everyone(x, axis), dim)


def over_copies(x, axis):
    return from_everyone(x, axis).sum(axis=0)


def in_one(arrays, axis):
    ends = [0]
    for a in arrays:
        ends.append(ends[-1] + a.size)
    running = over_copies(jnp.concatenate([a.ravel() for a in arrays]), axis)
    return tuple((running[b:e].reshape(a.shape) for a, b, e in zip(arrays, ends, ends[1:])))


def rms_scaled(values, gain):
    data = values.astype(jnp.float32)
    return data * lax.rsqrt(jnp.mean(data * data, axis=-1, keepdims=True) + 1e-06) * gain


def depthwise(padded, taps, length):
    wide = padded.astype(jnp.float32)
    conv = jnp.zeros((length, wide.shape[1]), jnp.float32)
    for offset in range(taps.shape[0]):
        conv = conv + taps[offset] * wide[offset : offset + length]
    return conv


def fetch_mlp(up_bf, down_bf):
    return gather_turned((up_bf, down_bf), "fs", (0, 1))


def shards(
    resid,
    norm1_gain,
    w_value,
    w_gate,
    value_scale,
    gate_scale,
    conv_taps,
    conv_gain,
    w_point,
    point_scale,
    norm2_gain,
    w_up,
    up_scale,
    w_down,
    down_scale,
):
    tok_rows = resid.shape[0]
    tp_count = lax.axis_size("tp")
    tp_rank = lax.axis_index("tp")
    seq_len = tok_rows * tp_count
    channels = value_scale.shape[0]
    group_width = channels // GROUPS
    reach = conv_taps.shape[0] // 2
    value_bf = w_value.astype(jnp.bfloat16)
    gate_bf = w_gate.astype(jnp.bfloat16)
    point_bf = w_point.astype(jnp.bfloat16)
    up_bf = w_up.astype(jnp.bfloat16)
    down_bf = w_down.astype(jnp.bfloat16)
    point_full, down_full = gather_turned((point_scale, down_scale), "fs", (0, 0))
    normed = rms_scaled(resid, norm1_gain).astype(jnp.bfloat16)
    value_rows, gate_rows, point_rows = gather_turned(
        (value_bf, gate_bf, point_bf), "fs", (0, 0, 1)
    )
    own_width = value_rows.shape[1]
    first = tp_rank * own_width
    own_value_scale = lax.dynamic_slice_in_dim(value_scale, first, own_width, 0)
    own_gate_scale = lax.dynamic_slice_in_dim(gate_scale, first, own_width, 0)
    own_taps = lax.dynamic_slice_in_dim(conv_taps, first, own_width, 1)
    own_gain = lax.dynamic_slice_in_dim(conv_gain, first, own_width, 0)
    piece = gather_directly(normed, "tp", 0)
    value = jnp.dot(piece, value_rows, preferred_element_type=jnp.float32) * own_value_scale
    gate = jnp.dot(piece, gate_rows, preferred_element_type=jnp.float32) * own_gate_scale
    glu_seq = (value * jax.nn.sigmoid(gate)).astype(jnp.bfloat16)
    padded = jnp.pad(glu_seq, ((reach, reach), (0, 0)))
    conv = depthwise(padded, own_taps, seq_len)
    member = ((first + jnp.arange(own_width)) % GROUPS)[:, None] == jnp.arange(GROUPS)[None, :]
    member = member.astype(jnp.float32)
    sums = jnp.dot(conv, member, precision=lax.Precision.HIGHEST)
    squares = jnp.dot(conv * conv, member, precision=lax.Precision.HIGHEST)
    totals, square_totals = in_one((sums, squares), "tp")
    gmean = jnp.dot(totals / group_width, member.T, precision=lax.Precision.HIGHEST)
    gsquare = jnp.dot(square_totals / group_width, member.T, precision=lax.Precision.HIGHEST)
    scaled = (conv - gmean) * lax.rsqrt(gsquare - gmean * gmean + 1e-05) * own_gain
    act = jax.nn.silu(scaled).astype(jnp.bfloat16)
    mixed = lax.psum_scatter(
        jnp.dot(act, point_rows, preferred_element_type=jnp.float32) * point_full,
        "tp",
        scatter_dimension=0,
        tiled=True,
    )
    middle = (resid.astype(jnp.float32) + mixed).astype(jnp.bfloat16)
    normed2 = rms_scaled(middle, norm2_gain).astype(jnp.bfloat16)
    up_cols, down_part = fetch_mlp(up_bf, down_bf)
    upper = (
        jnp.dot(gather_directly(normed2, "tp", 0), up_cols, preferred_element_type=jnp.float32)
        * up_scale
    )
    hidden = jnp.square(jax.nn.relu(upper)).astype(jnp.bfloat16)
    total = lax.psum_scatter(
        (jnp.dot(hidden, down_part, preferred_element_type=jnp.float32) * down_full).astype(
            jnp.bfloat16
        ),
        "tp",
        scatter_dimension=0,
        tiled=True,
    ).astype(jnp.float32)
    return (middle.astype(jnp.float32) + total).astype(jnp.bfloat16)


def solution(mesh):
    in_specs = (
        P(("fs", "tp"), None),
        P(),
        P("fs", "tp"),
        P("fs", "tp"),
        P(),
        P(),
        P(),
        P(),
        P("tp", "fs"),
        P("fs"),
        P(),
        P("fs", "tp"),
        P("tp"),
        P("tp", "fs"),
        P("fs"),
    )
    out_specs = P(("fs", "tp"), None)
    return jax.shard_map(shards, mesh=mesh, in_specs=in_specs, out_specs=out_specs, check_vma=False)
```

profile of v0, /device:TPU:1, one launch (start us, length us, event | category | flops | bytes accessed | tf_op | source)
XLA Modules:
  0.0 365.7 jit_solution(16230646207649153275)
XLA Ops:
  6.5 1.0 convert_bitcast_fusion.1
  7.5 1.0 copy.29
  8.5 1.0 copy.30
  9.6 0.7 pad_maximum_fusion.1
  10.3 0.0 all-gather.3.cloned.1.call-update
  10.3 0.2 fusion.16
  10.6 0.3 fusion.18
  10.8 3.5 broadcast_in_dim.6
  14.3 6.2 %all-to-all-start = ((bf16[8,192,2048]{2,1,0:T(8,128)(2,1)}), bf16[8,192,2048]{2,1,0:T(8,128)(2,1)}, u32[]{:S(2)}, u32[]{:S(2)}) async-start(bf16[8,192,2048]{2,1,0:T(8,128)(2,1)} %broadcast_in_dim.6), calls=%async_computation | async-start | bytes 12582912 | tf_op jit(solution)/shard_map/all_to_all | solution.py:28
  20.4 0.8 dynamic_slice.14
  21.2 0.8 dynamic_slice.13
  22.0 0.8 dynamic_slice.15
  22.7 21.5 %all_gather.10 = f32[2048,2]{0,1:T(2,128)S(1)} all-gather(f32[128,2]{0,1:T(2,128)S(1)} %pad_maximum_fusion.3), channel_id=1, replica_groups=mesh['fs'=16,'tp'=8] {'fs'}, dimensions={0}, use_global_device_ids=true | all-gather | bytes 17408 | tf_op jit(solution)/shard_map/all_gather | solution.py:12
  44.2 1.1 fusion.68
  45.3 1.2 constant_dynamic-slice_fusion
  46.5 45.2 %all-to-all-done = bf16[8,192,2048]{2,1,0:T(8,128)(2,1)} async-done(((bf16[8,192,2048]{2,1,0:T(8,128)(2,1)}), bf16[8,192,2048]{2,1,0:T(8,128)(2,1)}, u32[]{:S(2)}, u32[]{:S(2)}) %all-to-all-start) | async-done | bytes 6291488 | tf_op jit(solution)/shard_map/all_to_all | solution.py:28
  91.7 5.0 %fusion.14 = f32[1536,256]{1,0:T(8,128)S(1)} fusion(bf16[1536,2048]{1,0:T(8,128)(2,1)} %bitcast.1, bf16[2048,768]{0,1:T(8,128)(2,1)} %all-gather.3.cloned.1.call-done, f32[256]{0:T(256)S(1)} %dynamic_slice.14), kind=kOutput, calls=%fused_computation.18 | convolution fusion | flops 1612185600 | bytes 8913920 | tf_op jit(solution)/shard_map/dot_general | solution.py:106
  96.7 4.9 %fusion.15 = bf16[1536,256]{1,0:T(8,128)(2,1)S(1)} fusion(f32[1536,256]{1,0:T(8,128)S(1)} %fusion.14, bf16[1536,2048]{1,0:T(8,128)(2,1)} %bitcast.1, bf16[2048,768]{0,1:T(8,128)(2,1)} %all-gather.3.cloned.1.call-done, f32[256]{0:T(256)S(1)} %dynamic_slice.13), kind=kOutput, calls=%fused_computation.19 | convolution fusion | flops 1611792384 | bytes 9700352 | tf_op jit(solution)/shard_map/dot_general | solution.py:105
  101.6 0.2 pad_convert_fusion
  101.7 6.0 %fusion.24 = f32[1536,256]{1,0:T(8,128)S(1)} fusion(f32[1566,256]{1,0:T(8,128)S(1)} %pad_convert_fusion, f32[256]{0:T(256)S(1)} %bitcast.62, f32[256]{0:T(256)S(1)} %bitcast.64, f32[256]{0:T(256)S(1)} %bitcast.65, f32[256]{0:T(256)S(1)} %bitcast.66, f32[256]{0:T(256)S(1)} %bitcast.67, f32[256]{0:T(256)S(1)} %bitcast.68, f32[256]{0:T(256)S(1)} %bitcast.69, ...), kind=kLoop, calls=%fused_computation.35 | loop fusion | flops 23986176 | bytes 50363392 | tf_op jit(solution)/shard_map/add | solution.py:56
  107.8 1.8 fusion.60
  109.6 0.9 fusion.54
  110.5 1.6 reshape.84
  112.1 0.4 reshape.85
  112.5 0.9 broadcast_in_dim.7
  113.4 4.3 %all-to-all-start.1 = ((f32[8,1,12288]{2,1,0:T(1,128)}), f32[8,1,12288]{2,1,0:T(1,128)S(1)}, u32[]{:S(2)}, u32[]{:S(2)}) async-start(f32[8,1,12288]{2,1,0:T(1,128)} %broadcast_in_dim.7), calls=%async_computation.1 | async-start | bytes 786432 | tf_op jit(solution)/shard_map/all_to_all | solution.py:28
  117.8 7.7 %all-to-all-done.1 = f32[8,1,12288]{2,1,0:T(1,128)S(1)} async-done(((f32[8,1,12288]{2,1,0:T(1,128)}), f32[8,1,12288]{2,1,0:T(1,128)S(1)}, u32[]{:S(2)}, u32[]{:S(2)}) %all-to-all-start.1) | async-done | bytes 393248 | tf_op jit(solution)/shard_map/all_to_all | solution.py:28
  125.5 0.3 reduce_sum.28
  125.8 0.8 div.26
  126.6 2.0 fusion.59
  128.6 0.8 div.28
  129.4 2.7 multiply_convert_fusion.2
  132.2 7.6 %convolution_multiply_fusion = f32[1536,2048]{1,0:T(8,128)} fusion(bf16[1536,256]{1,0:T(8,128)(2,1)S(1)} %multiply_convert_fusion.2, f32[2048]{0:T(1024)S(1)} %bitcast.48, bf16[2048,768]{0,1:T(8,128)(2,1)} %all-gather.3.cloned.1.call-done), kind=kOutput, calls=%fused_computation.1 | convolution fusion | flops 1613758464 | bytes 14426112 | tf_op jit(solution)/shard_map/dot_general | solution.py:120
  139.7 0.0 all-gather.5.cloned.1.call-start
  139.8 1.0 copy-done.1
  140.7 0.2 copy.34
  141.0 0.8 pad_maximum_fusion
  141.8 0.0 all-gather.5.cloned.1.call-update
  141.8 71.1 %reduce-scatter.3.cloned.1.call-done = f32[192,2048]{1,0:T(8,128)} async-done(((f32[1536,2048]{1,0:T(8,128)}), f32[192,2048]{1,0:T(8,128)}) %reduce-scatter.3.cloned.1.call-update) | async-done | bytes 1572880 | tf_op jit(solution)/shard_map/reduce_scatter | solution.py:119
  212.9 1.7 fusion.20
  214.6 0.3 fusion.22
  214.9 3.5 broadcast_in_dim.8
  218.4 6.0 %all-to-all-start.2 = ((bf16[8,192,2048]{2,1,0:T(8,128)(2,1)}), bf16[8,192,2048]{2,1,0:T(8,128)(2,1)}, u32[]{:S(2)}, u32[]{:S(2)}) async-start(bf16[8,192,2048]{2,1,0:T(8,128)(2,1)} %broadcast_in_dim.8), calls=%async_computation.3 | async-start | bytes 12582912 | tf_op jit(solution)/shard_map/all_to_all | solution.py:28
  224.3 66.9 %all-gather.5.cloned.1.call-done = bf16[2048,2048]{0,1:T(8,128)(2,1)} async-done(((bf16[128,2048]{0,1:T(8,128)(2,1)}), bf16[2048,2048]{0,1:T(8,128)(2,1)}) %all-gather.5.cloned.1.call-update) | async-done | bytes 8388624 | tf_op jit(solution)/shard_map/all_gather | solution.py:12
  291.2 4.4 %all-to-all-done.2 = bf16[8,192,2048]{2,1,0:T(8,128)(2,1)} async-done(((bf16[8,192,2048]{2,1,0:T(8,128)(2,1)}), bf16[8,192,2048]{2,1,0:T(8,128)(2,1)}, u32[]{:S(2)}, u32[]{:S(2)}) %all-to-all-start.2) | async-done | bytes 6291488 | tf_op jit(solution)/shard_map/all_to_all | solution.py:28
  295.6 19.4 %multiply_convert_fusion = bf16[1536,2048]{1,0:T(8,128)(2,1)} fusion(f32[2048]{0:T(1024)S(1)} %bitcast.49, bf16[2048,2048]{0,1:T(8,128)(2,1)} %all-gather.5.cloned.1.call-done, bf16[1536,2048]{1,0:T(8,128)(2,1)} %bitcast.36, f32[1024]{0:T(1024)S(1)} %copy-done.7), kind=kOutput, calls=%fused_computation | convolution fusion | flops 12897484800 | bytes 20983808 | tf_op jit(solution)/shard_map/dot_general | solution.py:134
  315.1 41.8 %reduce-scatter.5.cloned.1.call-done = bf16[192,2048]{1,0:T(8,128)(2,1)} async-done(((bf16[1536,2048]{1,0:T(8,128)(2,1)}), bf16[192,2048]{1,0:T(8,128)(2,1)}) %reduce-scatter.5.cloned.1.call-update) | async-done | bytes 786448 | tf_op jit(solution)/shard_map/reduce_scatter | solution.py:133
  356.9 2.3 fusion.23
  (29 shorter events, 0.2 us)
Async XLA Ops:
  6.5 3.8 %copy-start = (bf16[192,2048]{1,0:T(8,128)(2,1)S(1)}, bf16[192,2048]{1,0:T(8,128)(2,1)}, u32[]{:S(2)}) copy-start(bf16[192,2048]{1,0:T(8,128)(2,1)} %param.15) | copy-start | bytes 2359300
  6.5 4.0 %copy-start.3 = (f32[2048]{0:T(1024)S(1)}, f32[2048]{0:T(1024)}, u32[]{:S(2)}) copy-start(f32[2048]{0:T(1024)} %param.16) | copy-start | bytes 24580
  6.5 85.2 %all-gather.3.cloned.1.call-start = ((), (), s32[]{:S(2)}) async-start(), calls=%async_computation.5 | async-start | bytes 3342336 | tf_op jit(solution)/shard_map/all_gather | solution.py:12
  14.3 8.4 %copy-start.5 = (f32[128]{0:T(128)S(1)}, f32[128]{0:T(128)}, u32[]{:S(2)}) copy-start(f32[128]{0:T(128)} %param.29) | copy-start | bytes 1540
  14.3 8.4 %copy-start.6 = (f32[128]{0:T(128)S(1)}, f32[128]{0:T(128)}, u32[]{:S(2)}) copy-start(f32[128]{0:T(128)} %param.24) | copy-start | bytes 1540
  14.3 77.4 %all-to-all-start = ((bf16[8,192,2048]{2,1,0:T(8,128)(2,1)}), bf16[8,192,2048]{2,1,0:T(8,128)(2,1)}, u32[]{:S(2)}, u32[]{:S(2)}) async-start(bf16[8,192,2048]{2,1,0:T(8,128)(2,1)} %broadcast_in_dim.6), calls=%async_computation | async-start | bytes 12582912 | tf_op jit(solution)/shard_map/all_to_all | solution.py:28
  113.4 12.0 %all-to-all-start.1 = ((f32[8,1,12288]{2,1,0:T(1,128)}), f32[8,1,12288]{2,1,0:T(1,128)S(1)}, u32[]{:S(2)}, u32[]{:S(2)}) async-start(f32[8,1,12288]{2,1,0:T(1,128)} %broadcast_in_dim.7), calls=%async_computation.1 | async-start | bytes 786432 | tf_op jit(solution)/shard_map/all_to_all | solution.py:28
  117.8 95.2 %reduce-scatter.3.cloned.1.call-start = ((), (), s32[]{:S(2)}) async-start(), calls=%async_computation.6 | async-start | bytes 14155776 | tf_op jit(solution)/shard_map/reduce_scatter | solution.py:119
  139.7 1.0 copy-start.1
  139.7 1.2 copy-start.2
  139.7 151.5 %all-gather.5.cloned.1.call-start = ((), (), s32[]{:S(2)}) async-start(), calls=%async_computation.7 | async-start | bytes 8912896 | tf_op jit(solution)/shard_map/all_gather | solution.py:12
  141.8 72.8 %copy-start.4 = (f32[2048]{0:T(1024)S(1)}, f32[2048]{0:T(1024)}, u32[]{:S(2)}) copy-start(f32[2048]{0:T(1024)} %param.25) | copy-start | bytes 24580
  218.4 77.2 %copy-start.7 = (f32[1024]{0:T(1024)S(1)}, f32[1024]{0:T(1024)}, u32[]{:S(2)}) copy-start(f32[1024]{0:T(1024)} %param.27) | copy-start | bytes 12292
  218.4 77.2 %all-to-all-start.2 = ((bf16[8,192,2048]{2,1,0:T(8,128)(2,1)}), bf16[8,192,2048]{2,1,0:T(8,128)(2,1)}, u32[]{:S(2)}, u32[]{:S(2)}) async-start(bf16[8,192,2048]{2,1,0:T(8,128)(2,1)} %broadcast_in_dim.8), calls=%async_computation.3 | async-start | bytes 12582912 | tf_op jit(solution)/shard_map/all_to_all | solution.py:28
  224.3 132.6 %reduce-scatter.5.cloned.1.call-start = ((), (), s32[]{:S(2)}) async-start(), calls=%async_computation.8 | async-start | bytes 7077888 | tf_op jit(solution)/shard_map/reduce_scatter | solution.py:133
Sparse Core Ops, SparseCore 0:
  10.4 53.8 all-gather.2
  139.9 73.0 reduce-scatter.2
  215.0 76.1 all-gather.4
  315.2 41.6 reduce-scatter.4
where the time goes:
time: 367 us; the launch traced here: 366 us
  waiting for transfers between devices  237 us (65%)
  matrix products  44.3 us (12%)
  blocking collectives  21.5 us (6%)
  local copies, waits for them, and re-layouts  19.2 us (5%)
  starting transfers between devices  16.5 us (4%)
  other arithmetic  13.8 us (4%)
  between operations  13.3 us (4%)
    reduce_scatter x1, waiting for transfers between devices, shards(): lax.psum_scatter(jnp.dot(act, point_rows, preferred_element_type=jnp.floa...  71.1 us
    all_gather x2, waiting for transfers between devices, gather_turned(): result, at, done = (lax.all_gather(both, axis, axis=0, tiled=True), 0, [])  66.9 us
    all_to_all x3, waiting for transfers between devices, from_everyone(): return lax.all_to_all(copies, axis, split_axis=0, concat_axis=0, tiled=True)  57.3 us
    reduce_scatter x1, waiting for transfers between devices, shards(): lax.psum_scatter((jnp.dot(hidden, down_part, preferred_element_type=jnp.f...  41.8 us
    all_gather x1, blocking collectives, gather_turned(): result, at, done = (lax.all_gather(both, axis, axis=0, tiled=True), 0, [])  21.5 us
    dot_general x1, matrix products, shards(): jnp.dot(hidden, down_part, preferred_element_type=jnp.float32) * down_full  19.4 us
    all_to_all x3, starting transfers between devices, from_everyone(): return lax.all_to_all(copies, axis, split_axis=0, concat_axis=0, tiled=True)  16.4 us
    broadcast_in_dim x3, local copies, waits for them, and re-layouts, from_everyone(): copies = jnp.broadcast_to(x, (lax.axis_size(axis), *x.shape))  7.88 us
  transfers between devices with their start and end apart: 7, of which 6 were waited for; matrix products, arithmetic and copies ran while one was open for 4% of the time, Pallas kernels for 0%

commit v1 on v0

v1 whole, which is shorter than its diff:
```python
import functools

import jax
import jax.numpy as jnp
from jax import lax
from jax.experimental import pallas as pl
from jax.experimental.pallas import tpu as pltpu
from jax.sharding import PartitionSpec as P

BF = jnp.bfloat16
F32 = jnp.float32
MESH = pl.DeviceIdType.MESH

RB = 192
HB = 96
CB = 384
SEQ = 1536
D = 2048
CW = 256
HALO = 16
KERNEL = 31
GROUP_WIDTH = 512.0
N_SEM = 120


def dot(a, b):
    return jnp.dot(a, b, preferred_element_type=F32)


class Copies:
    def __init__(self, send, recv):
        self.send, self.recv, self.used, self.started = send, recv, 0, []

    def take(self, count=1):
        at = self.used
        self.used += count
        assert self.used <= N_SEM
        return at

    def copy(self, src, dst, device, at=None):
        at = self.take() if at is None else at
        return pltpu.make_async_remote_copy(
            src_ref=src,
            dst_ref=dst,
            send_sem=self.send.at[at],
            recv_sem=self.recv.at[at],
            device_id=device,
            device_id_type=MESH,
        )

    def start(self, src, dst, device):
        made = self.copy(src, dst, device)
        made.start()
        self.started.append(made)
        return made

    def finish(self):
        for made in self.started:
            made.wait_send()


def kernel(
    resid,
    gain1,
    w_value,
    w_gate,
    value_scale,
    gate_scale,
    taps,
    conv_gain,
    w_point,
    point_scale,
    gain2,
    w_up,
    up_scale,
    w_down,
    down_scale,
    out,
    x1,
    x2,
    vg,
    pp,
    uu,
    dd,
    glu,
    cin,
    cv,
    st,
    st_in,
    act,
    mix_out,
    mix_in,
    mix,
    mid,
    hid,
    par_out,
    par_in,
    par,
    rel_in,
    fin_in,
    send_sem,
    recv_sem,
):
    fs = lax.axis_index("fs")
    tp = lax.axis_index("tp")
    z, y = fs // 4, fs % 4
    x, c = tp // 2, tp % 2
    xp, xm, xf = (x + 1) % 4, (x + 3) % 4, (x + 2) % 4
    yp, ym = (y + 1) % 4, (y + 3) % 4
    zp, zm = (z + 1) % 4, (z + 3) % 4
    to_xp, to_xm, to_xf = ({"tp": v * 2 + c} for v in (xp, xm, xf))
    to_pair = {"tp": x * 2 + 1 - c}
    to_yp, to_ym = ({"fs": z * 4 + v} for v in (yp, ym))
    to_zp, to_zm = ({"fs": v * 4 + y} for v in (zp, zm))
    cp = Copies(send_sem, recv_sem)

    barrier = pltpu.get_barrier_semaphore()
    for peer in (to_pair, to_xp, to_xm, to_xf, to_yp, to_ym, to_zp, to_zm):
        pl.semaphore_signal(barrier, inc=1, device_id=peer, device_id_type=MESH)

    vg[0, z, y] = w_value[...].astype(BF)
    vg[1, z, y] = w_gate[...].astype(BF)
    own_point = pp.at[x // 2, z, y, pl.ds(pl.multiple_of((x % 2) * 256, 256), 256)]
    own_point[...] = (w_point[...] * point_scale[...]).astype(BF)
    for half in range(2):
        uu[half, z, y] = w_up[:, half * 512 : half * 512 + 512].astype(BF)
        dd[half, z, y] = (w_down[half * 512 : half * 512 + 512, :] * down_scale[...]).astype(BF)

    def norm_rows(source, gain, target, base):
        def step(i, carry):
            rows = pl.multiple_of(i * 16, 16)
            v = source[pl.ds(rows, 16), :].astype(F32)
            scale = lax.rsqrt(jnp.mean(v * v, axis=-1, keepdims=True) + 1e-06)
            at = pl.multiple_of(base + i * 16, 16)
            target[pl.ds(at, 16), :] = (v * scale * gain[...]).astype(BF)
            return carry

        lax.fori_loop(0, RB // 16, step, 0)

    norm_rows(resid, gain1, x1, tp * RB)
    pl.semaphore_wait(barrier, 8)

    class Ring:
        def __init__(self, buf):
            self.buf = buf

        def at(self, v, core, first, count):
            return self.buf.at[pl.ds(pl.multiple_of(v * CB + core * RB + first, 16), count)]

        def own(self):
            lo, hi = self.at(x, c, 0, HB), self.at(x, c, HB, HB)
            whole = self.at(x, c, 0, RB)
            self.p0 = cp.start(lo, lo, to_xp)
            self.m1 = cp.start(hi, hi, to_xm)
            self.p1 = cp.start(hi, hi, to_xp)
            self.m0 = cp.start(lo, lo, to_xm)
            self.d0 = cp.start(whole, whole, to_pair)

        def relay(self):
            self.p0.wait_recv()
            lo = self.at(xm, c, 0, HB)
            self.rp = cp.start(lo, lo, to_xp)
            self.d1 = cp.start(lo, lo, to_pair)
            self.m1.wait_recv()
            hi = self.at(xp, c, HB, HB)
            self.rm = cp.start(hi, hi, to_xm)
            self.d2 = cp.start(hi, hi, to_pair)

        def near(self):
            self.p1.wait_recv()
            hi = self.at(xm, c, HB, HB)
            self.d3 = cp.start(hi, hi, to_pair)
            self.m0.wait_recv()
            lo = self.at(xp, c, 0, HB)
            self.d4 = cp.start(lo, lo, to_pair)

        def near_wait(self):
            for made in (self.d1, self.d2, self.d3, self.d4):
                made.wait_recv()

        def far(self):
            self.rp.wait_recv()
            lo = self.at(xf, c, 0, HB)
            self.d5 = cp.start(lo, lo, to_pair)
            self.rm.wait_recv()
            hi = self.at(xf, c, HB, HB)
            self.d6 = cp.start(hi, hi, to_pair)

        def far_wait(self):
            self.d5.wait_recv()
            self.d6.wait_recv()

    class Weights:
        def __init__(self, buf):
            self.buf, self.deep = buf, buf.shape[3]

        def s0(self):
            a, b = self.buf.at[0, z, y], self.buf.at[1, z, y]
            self.first = [
                cp.start(a, a, to_yp),
                cp.start(b, b, to_zp),
                cp.start(a, a, to_ym),
                cp.start(b, b, to_zm),
            ]

        def s1(self):
            half = self.deep // 2
            lo, hi = pl.ds(0, half), pl.ds(half, half)
            plan = (
                (self.buf.at[0, z, ym, lo], to_yp),
                (self.buf.at[1, zm, y, lo], to_zp),
                (self.buf.at[0, z, yp, hi], to_ym),
                (self.buf.at[1, zp, y, hi], to_zm),
            )
            self.second = []
            for made, (ref, peer) in zip(self.first, plan):
                made.wait_recv()
                self.second.append(cp.start(ref, ref, peer))

        def s2(self):
            for made in self.second:
                made.wait_recv()
            a, b = self.buf.at[0, z], self.buf.at[1, :, y]
            self.third = [
                cp.start(a, a, to_zp),
                cp.start(b, b, to_yp),
                cp.start(a, a, to_zm),
                cp.start(b, b, to_ym),
            ]

        def s3(self):
            lo, hi = pl.ds(0, 2), pl.ds(2, 2)
            plan = (
                (self.buf.at[0, zm, lo], to_zp),
                (self.buf.at[1, lo, ym], to_yp),
                (self.buf.at[0, zp, hi], to_zm),
                (self.buf.at[1, hi, yp], to_ym),
            )
            self.fourth = []
            for made, (ref, peer) in zip(self.third, plan):
                made.wait_recv()
                self.fourth.append(cp.start(ref, ref, peer))

        def s4(self):
            for made in self.fourth:
                made.wait_recv()

    ring1, ring2 = Ring(x1), Ring(x2)
    gv, gp, gu, gd = Weights(vg), Weights(pp), Weights(uu), Weights(dd)

    gv.s0()
    point_x = [cp.start(own_point, own_point, peer) for peer in (to_xp, to_xm, to_xf)]
    ring1.own()
    gv.s1()
    gv.s2()
    for made in point_x:
        made.wait_recv()
    gp.s0()

    glu[0:HALO, :] = jnp.zeros((HALO, CW), BF)
    glu[HALO + SEQ : HALO + SEQ + HALO, :] = jnp.zeros((HALO, CW), BF)
    st[...] = jnp.zeros(st.shape, F32)

    ring1.relay()
    gp.s1()
    gv.s3()
    gp.s2()
    gu.s0()

    own_cols = pl.ds(pl.multiple_of(tp * CW, CW), CW)

    def gated(v):
        rows = pl.multiple_of(v * CB, CB)
        block = x1[pl.ds(rows, CB), :]
        value = dot(block, vg[0].reshape(D, CW)) * value_scale[:, own_cols]
        gate = dot(block, vg[1].reshape(D, CW)) * gate_scale[:, own_cols]
        glu[pl.ds(pl.multiple_of(rows + HALO, 16), CB), :] = (value * jax.nn.sigmoid(gate)).astype(BF)

    ring1.d0.wait_recv()
    gv.s4()
    gated(x)
    ring1.near()
    ring1.near_wait()
    gated(xp)
    gated(xm)
    ring1.far()
    ring1.far_wait()
    gated(xf)

    def glu_for(v):
        return glu.at[pl.ds(pl.multiple_of(v * CB, CB), CB + 2 * HALO)]

    sent_glu = [cp.start(glu_for(v), cin.at[x], peer) for v, peer in ((xf, to_xf), (xp, to_xp), (xm, to_xm))]
    cin[x] = glu_for(x)[...]

    def convolve(v):
        def step(i, carry):
            part, chunk = i % 2, i // 2
            lane = pl.multiple_of(part * 128, 128)
            row = pl.multiple_of(chunk * 64, 64)
            col = pl.multiple_of((2 * v + c) * CW + part * 128, 128)
            data = cin[v, pl.ds(row, 96), pl.ds(lane, 128)].astype(F32)
            total = jnp.zeros((64, 128), F32)
            for b in range(8):
                turned = data if b == 0 else pltpu.roll(data, 96 - b, 0)
                for a in range(4):
                    k = 8 * a + b
                    if k:
                        tap = taps[k - 1 : k, pl.ds(col, 128)]
                        total = total + tap * turned[8 * a : 8 * a + 64]
            cv[v, pl.ds(row, 64), pl.ds(lane, 128)] = total
            st[0, pl.ds(row, 64), :] += total
            st[1, pl.ds(row, 64), :] += total * total
            return carry

        lax.fori_loop(0, 12, step, 0)

    convolve(x)
    gp.s3()
    gu.s1()
    sent_glu[1].wait_recv()
    convolve(xm)
    sent_glu[2].wait_recv()
    convolve(xp)
    sent_glu[0].wait_recv()
    convolve(xf)

    for kind in range(2):
        total = st[kind]
        for shift in (4, 8, 16, 32, 64):
            total = total + pltpu.roll(total, shift, 1)
        st[kind] = total
    sent_stats = cp.start(st, st_in, to_pair)
    gp.s4()
    gu.s2()
    gd.s0()
    sent_stats.wait_recv()

    def activate(i, carry):
        rows = pl.ds(pl.multiple_of(i * 32, 32), 32)
        gmean = (st[0, rows, :] + st_in[0, rows, :]) / GROUP_WIDTH
        gsquare = (st[1, rows, :] + st_in[1, rows, :]) / GROUP_WIDTH
        inv = lax.rsqrt(gsquare - gmean * gmean + 1e-05)
        for v in range(4):
            for part in range(2):
                col = pl.multiple_of((2 * v + c) * CW + part * 128, 128)
                lane = part * 128
                s = (cv[v, rows, lane : lane + 128] - gmean) * inv * conv_gain[:, pl.ds(col, 128)]
                act[rows, v * CW + lane : v * CW + lane + 128] = (s / (1.0 + jnp.exp(-s))).astype(BF)
        return carry

    lax.fori_loop(0, CB // 32, activate, 0)

    pair_rows = pl.ds(pl.multiple_of((1 - c) * RB, RB), RB)
    own_rows = pl.ds(pl.multiple_of(c * RB, RB), RB)
    mix_at = cp.take(8)

    def mix_copy(n):
        return cp.copy(mix_out.at[n], mix_in.at[n], to_pair, mix_at + n)

    def columns(buf, half, n):
        two = buf[half, n // 2, pl.ds((n % 2) * 2, 2)]
        return jnp.concatenate([two[0], two[1]], axis=1)

    def point(n, carry):
        left = jnp.concatenate([act[pair_rows, 0:512], act[own_rows, 0:512]], axis=0)
        right = jnp.concatenate([act[pair_rows, 512:1024], act[own_rows, 512:1024]], axis=0)
        both = dot(left, columns(pp, 0, n)) + dot(right, columns(pp, 1, n))
        mix_out[n] = both[:RB].astype(BF)
        mix_copy(n).start()
        mix[:, pl.ds(pl.multiple_of(n * 256, 256), 256)] = both[RB:]
        return carry

    lax.fori_loop(0, 8, point, 0)

    def add_mixed(n, carry):
        mix_copy(n).wait_recv()
        cols = pl.ds(pl.multiple_of(n * 256, 256), 256)
        mixed = mix[:, cols] + mix_in[n].astype(F32)
        mid[:, cols] = (resid[:, cols].astype(F32) + mixed).astype(BF)
        return carry

    lax.fori_loop(0, 8, add_mixed, 0)
    norm_rows(mid, gain2, x2, tp * RB)
    ring2.own()
    gu.s3()
    gd.s1()

    def up(v):
        rows = pl.ds(pl.multiple_of(v * CB, CB), CB)

        def step(n, carry):
            weight = uu[n // 2, :, :, :, pl.ds(pl.multiple_of((n % 2) * 256, 256), 256)].reshape(D, 256)
            cols = pl.ds(pl.multiple_of(n * 256, 256), 256)
            upper = jnp.maximum(dot(x2[rows, :], weight) * up_scale[:, cols], 0.0)
            hid[rows, cols] = (upper * upper).astype(BF)
            return carry

        lax.fori_loop(0, 4, step, 0)

    ring2.relay()
    gu.s4()
    gd.s2()
    ring2.d0.wait_recv()
    up(x)
    ring2.near()
    ring2.near_wait()
    up(xp)
    up(xm)
    ring2.far()
    gd.s3()
    ring2.far_wait()
    up(xf)
    gd.s4()

    def down(v):
        pair_at = pl.ds(pl.multiple_of(v * CB + (1 - c) * RB, RB), RB)
        own_at = pl.ds(pl.multiple_of(v * CB + c * RB, RB), RB)

        def step(n, carry):
            left = jnp.concatenate([hid[pair_at, 0:512], hid[own_at, 0:512]], axis=0)
            right = jnp.concatenate([hid[pair_at, 512:1024], hid[own_at, 512:1024]], axis=0)
            both = dot(left, columns(dd, 0, n)) + dot(right, columns(dd, 1, n))
            cols = pl.ds(pl.multiple_of(n * 256, 256), 256)
            par_out[v, :, cols] = both[:RB].astype(BF)
            par[v, :, cols] = both[RB:].astype(BF)
            return carry

        lax.fori_loop(0, 8, step, 0)
        return cp.start(par_out.at[v], par_in.at[v], to_pair)

    def add_pair(v, made, first=0, count=RB):
        made.wait_recv()

        def step(i, carry):
            rows = pl.ds(pl.multiple_of(i * 32, 32), 32)
            par[v, rows, :] = (par[v, rows, :].astype(F32) + par_in[v, rows, :].astype(F32)).astype(BF)
            return carry

        lax.fori_loop(0, RB // 32, step, 0)

    lo, hi = pl.ds(0, HB), pl.ds(HB, HB)
    made_f = down(xf)
    made_p = down(xp)
    add_pair(xf, made_f)
    relay_p = cp.start(par.at[xf, lo], rel_in.at[0], to_xp)
    relay_m = cp.start(par.at[xf, hi], rel_in.at[1], to_xm)
    made_m = down(xm)
    add_pair(xp, made_p)
    plain_p = cp.start(par.at[xp, hi], fin_in.at[0, hi], to_xp)
    add_pair(xm, made_m)
    plain_m = cp.start(par.at[xm, lo], fin_in.at[1, lo], to_xm)
    made_x = down(x)

    def add_relay(v, slot, first):
        def step(i, carry):
            rows = pl.ds(pl.multiple_of(first + i * 32, 32), 32)
            here = pl.ds(pl.multiple_of(i * 32, 32), 32)
            par[v, rows, :] = (par[v, rows, :].astype(F32) + rel_in[slot, here, :].astype(F32)).astype(BF)
            return carry

        lax.fori_loop(0, HB // 32, step, 0)

    relay_p.wait_recv()
    add_relay(xp, 0, 0)
    last_p = cp.start(par.at[xp, lo], fin_in.at[0, lo], to_xp)
    relay_m.wait_recv()
    add_relay(xm, 1, HB)
    last_m = cp.start(par.at[xm, hi], fin_in.at[1, hi], to_xm)

    made_x.wait_recv()

    def add_own(i, carry):
        rows = pl.ds(pl.multiple_of(i * 16, 16), 16)
        mix[rows, :] = mid[rows, :].astype(F32) + (par[x, rows, :].astype(F32) + par_in[x, rows, :].astype(F32))
        return carry

    lax.fori_loop(0, RB // 16, add_own, 0)
    for made in (plain_p, plain_m, last_p, last_m):
        made.wait_recv()

    def finish(i, carry):
        rows = pl.ds(pl.multiple_of(i * 16, 16), 16)
        total = fin_in[0, rows, :].astype(F32) + fin_in[1, rows, :].astype(F32)
        out[rows, :] = (mix[rows, :] + total).astype(BF)
        return carry

    lax.fori_loop(0, RB // 16, finish, 0)
    cp.finish()

    def mix_sent(n, carry):
        mix_copy(n).wait_send()
        return carry

    lax.fori_loop(0, 8, mix_sent, 0)


SCRATCH = (
    ((SEQ, D), BF),
    ((SEQ, D), BF),
    ((2, 4, 4, 128, 256), BF),
    ((2, 4, 4, 512, 128), BF),
    ((2, 4, 4, 128, 512), BF),
    ((2, 4, 4, 512, 128), BF),
    ((SEQ + 2 * HALO, CW), BF),
    ((4, CB + 2 * HALO, CW), BF),
    ((4, CB, CW), F32),
    ((2, CB, 128), F32),
    ((2, CB, 128), F32),
    ((CB, 4 * CW), BF),
    ((8, RB, 256), BF),
    ((8, RB, 256), BF),
    ((RB, D), F32),
    ((RB, D), BF),
    ((SEQ, 1024), BF),
    ((4, RB, D), BF),
    ((4, RB, D), BF),
    ((4, RB, D), BF),
    ((2, HB, D), BF),
    ((2, RB, D), BF),
)


def shards(*arrays):
    flat = [a.reshape(1, -1) if a.ndim == 1 else a for a in arrays]
    return pl.pallas_call(
        kernel,
        out_shape=jax.ShapeDtypeStruct((RB, D), BF),
        in_specs=[pl.BlockSpec(memory_space=pltpu.VMEM)] * len(flat),
        out_specs=pl.BlockSpec(memory_space=pltpu.VMEM),
        scratch_shapes=[pltpu.VMEM(shape, kind) for shape, kind in SCRATCH]
        + [pltpu.SemaphoreType.DMA((N_SEM,)), pltpu.SemaphoreType.DMA((N_SEM,))],
        compiler_params=pltpu.CompilerParams(
            collective_id=0, has_side_effects=True, vmem_limit_bytes=66 * 1000 * 1000
        ),
        name="layer",
    )(*flat)


def solution(mesh):
    in_specs = (
        P(("fs", "tp"), None),
        P(),
        P("fs", "tp"),
        P("fs", "tp"),
        P(),
        P(),
        P(),
        P(),
        P("tp", "fs"),
        P("fs"),
        P(),
        P("fs", "tp"),
        P("tp"),
        P("tp", "fs"),
        P("fs"),
    )
    out_specs = P(("fs", "tp"), None)
    return jax.shard_map(shards, mesh=mesh, in_specs=in_specs, out_specs=out_specs, check_vma=False)
```

time: 367 us -> 140 us (0.38)
  waiting for transfers between devices: 237 us -> 0 us
  Pallas kernels: 0 us -> 137 us
  matrix products: 44.3 us -> 0 us
  blocking collectives: 21.5 us -> 0 us
  local copies, waits for them, and re-layouts: 19.2 us -> 2.09 us
  starting transfers between devices: 16.5 us -> 0 us
  other arithmetic: 13.8 us -> 0 us
  between operations: 13.3 us -> 0.01 us
    pallas_call x0 -> x1, Pallas kernels: none -> 137 us  [shards(): pl.pallas_call(kernel, out_shape=jax.ShapeDtypeStruct((RB, D), BF), in_sp...]
    reduce_scatter x2 -> x0, waiting for transfers between devices: 113 us -> none  [the longest x1 71.1 us: shards(): lax.psum_scatter(jnp.dot(act, point_rows, preferred_element_type=jnp.floa...]
    all_gather x2 -> x0, waiting for transfers between devices: 66.9 us -> none  [gather_turned(): result, at, done = (lax.all_gather(both, axis, axis=0, tiled=True), 0, [])]
    all_to_all x3 -> x0, waiting for transfers between devices: 57.3 us -> none  [from_everyone(): return lax.all_to_all(copies, axis, split_axis=0, concat_axis=0, tiled=True)]
    dot_general x8 -> x0, matrix products: 44.3 us -> none  [the longest x1 19.4 us: shards(): jnp.dot(hidden, down_part, preferred_element_type=jnp.float32) * down_full]
    all_gather x1 -> x0, blocking collectives: 21.5 us -> none  [gather_turned(): result, at, done = (lax.all_gather(both, axis, axis=0, tiled=True), 0, [])]
    all_to_all x3 -> x0, starting transfers between devices: 16.4 us -> none  [from_everyone(): return lax.all_to_all(copies, axis, split_axis=0, concat_axis=0, tiled=True)]
    broadcast_in_dim x3 -> x0, local copies, waits for them, and re-layouts: 7.88 us -> none  [from_everyone(): copies = jnp.broadcast_to(x, (lax.axis_size(axis), *x.shape))]
  transfers between devices with their start and end apart: 7 -> 0, of which waited for: 6 -> 0; matrix products, arithmetic and copies ran while one was open for 4% -> 0% of each run, Pallas kernels for 0% -> 0%
where the time goes in v1:
time: 140 us; the launch traced here: 139 us
  Pallas kernels  137 us (98%)
  local copies, waits for them, and re-layouts  2.09 us (1%)
    pallas_call x1, Pallas kernels, shards(): pl.pallas_call(kernel, out_shape=jax.ShapeDtypeStruct((RB, D), BF), in_sp...  137 us

profile of v1, /device:TPU:1, one launch (start us, length us, event | category | flops | bytes accessed | tf_op | source)
XLA Modules:
  0.0 138.9 jit_solution(9007414186080030190)
XLA Ops:
  0.0 136.8 %layer.1 = bf16[192,2048]{1,0:T(8,128)(2,1)} custom-call(bf16[192,2048]{1,0:T(8,128)(2,1)} %resid.1, f32[1,2048]{1,0:T(1,128)} %bitcast.8, f32[128,256]{1,0:T(8,128)} %w_value.1, f32[128,256]{1,0:T(8,128)} %w_gate.1, f32[1,2048]{1,0:T(1,128)} %bitcast.9, f32[1,2048]{1,0:T(1,128)} %bitcast.10, f32[31,2048]{1,0:T(8,128)} %taps.1, f32[1,2048]{1,0:T(1,128)} %bitcast.11, ...), custom_call_target="tpu_custom_call" | custom-call | tf_op jit(solution)/shard_map/layer/pallas_call | solution.py:526
  136.8 2.1 %copy.17 = bf16[192,2048]{1,0:T(8,128)(2,1)} copy(bf16[192,2048]{1,0:T(8,128)(2,1)} %layer.1) | data formatting | bytes 1572864

commit v2 on v1

v2 whole, which is shorter than its diff:
```python
import functools

import jax
import jax.numpy as jnp
from jax import lax
from jax.experimental import pallas as pl
from jax.experimental.pallas import tpu as pltpu
from jax.sharding import PartitionSpec as P

BF = jnp.bfloat16
F32 = jnp.float32
MESH = pl.DeviceIdType.MESH

RB = 192
QB = 48
CB = 384
SEQ = 1536
D = 2048
CW = 256
HALO = 16
FAR = 208
KERNEL = 31
GROUP_WIDTH = 512.0
N_SEM = 260

ORDER = (
    "V.s0", "D.s0", "px.0", "R1.oa", "c.init", "px.1", "V.s1", "R1.ob", "U.s0", "V.s2", "R1.oc", "U.s1",
    "R1.ra", "px.2", "V.s3", "P.s0", "R1.rb", "V.s4", "R1.nr", "P.s1", "D.s1", "c.gx", "P.s2", "R1.nw",
    "c.gp", "R1.fa", "c.sp", "c.gm", "R1.fb", "R1.fw", "c.gf", "P.s3", "c.cx", "c.fr", "U.s2", "c.cm", "c.cp",
    "c.cf", "c.st", "P.s4", "c.ac", "c.pt", "c.nm", "R2.oa", "U.s3", "R2.ob", "R2.oc", "D.s2", "R2.ra",
    "D.s3", "U.s4", "c.ux", "R2.rb", "R2.nr", "R2.nw", "c.up", "R2.fa", "c.um", "D.s4", "d.pl", "R2.fb",
    "R2.fw", "c.uf", "d.fa", "d.la", "d.sl", "d.xx", "d.fn",
)


def dot(a, b):
    return jnp.dot(a, b, preferred_element_type=F32)


class Copies:
    def __init__(self, send, recv):
        self.send, self.recv, self.used, self.started = send, recv, 0, []

    def take(self, count=1):
        at = self.used
        self.used += count
        assert self.used <= N_SEM
        return at

    def copy(self, src, dst, device, at=None):
        at = self.take() if at is None else at
        return pltpu.make_async_remote_copy(
            src_ref=src,
            dst_ref=dst,
            send_sem=self.send.at[at],
            recv_sem=self.recv.at[at],
            device_id=device,
            device_id_type=MESH,
        )

    def start(self, src, dst, device):
        made = self.copy(src, dst, device)
        made.start()
        self.started.append(made)
        return made

    def finish(self):
        for made in self.started:
            made.wait_send()


def kernel(
    resid,
    gain1,
    w_value,
    w_gate,
    value_scale,
    gate_scale,
    taps,
    conv_gain,
    w_point,
    point_scale,
    gain2,
    w_up,
    up_scale,
    w_down,
    down_scale,
    out,
    x1,
    x2,
    vg,
    pp,
    uu,
    dd,
    glu,
    cin,
    cv,
    st,
    st_in,
    act,
    mix_out,
    mix_in,
    mix,
    mid,
    hid,
    par_out,
    par_in,
    par,
    rel_in,
    fin_in,
    far_in,
    out_buf,
    send_sem,
    recv_sem,
):
    fs = lax.axis_index("fs")
    tp = lax.axis_index("tp")
    z, y = fs // 4, fs % 4
    x, c = tp // 2, tp % 2
    xp, xm, xf = (x + 1) % 4, (x + 3) % 4, (x + 2) % 4
    yp, ym = (y + 1) % 4, (y + 3) % 4
    zp, zm = (z + 1) % 4, (z + 3) % 4
    to_xp, to_xm, to_xf = ({"tp": v * 2 + c} for v in (xp, xm, xf))
    to_pair = {"tp": x * 2 + 1 - c}
    to_yp, to_ym = ({"fs": z * 4 + v} for v in (yp, ym))
    to_zp, to_zm = ({"fs": v * 4 + y} for v in (zp, zm))
    cp = Copies(send_sem, recv_sem)

    barrier = pltpu.get_barrier_semaphore()
    for peer in (to_pair, to_xp, to_xm, to_xf, to_yp, to_ym, to_zp, to_zm):
        pl.semaphore_signal(barrier, inc=1, device_id=peer, device_id_type=MESH)

    vg[0, z, y] = w_value[...].astype(BF)
    vg[1, z, y] = w_gate[...].astype(BF)
    own_point = pp.at[x // 2, z, y, pl.ds(pl.multiple_of((x % 2) * 256, 256), 256)]
    own_point[...] = (w_point[...] * point_scale[...]).astype(BF)
    for half in range(2):
        uu[half, z, y] = w_up[:, half * 512 : half * 512 + 512].astype(BF)
        dd[half, z, y] = (w_down[half * 512 : half * 512 + 512, :] * down_scale[...]).astype(BF)

    def norm_rows(source, gain, target, base):
        def step(i, carry):
            rows = pl.multiple_of(i * 16, 16)
            v = source[pl.ds(rows, 16), :].astype(F32)
            scale = lax.rsqrt(jnp.mean(v * v, axis=-1, keepdims=True) + 1e-06)
            at = pl.multiple_of(base + i * 16, 16)
            target[pl.ds(at, 16), :] = (v * scale * gain[...]).astype(BF)
            return carry

        lax.fori_loop(0, RB // 16, step, 0)

    norm_rows(resid, gain1, x1, tp * RB)
    pl.semaphore_wait(barrier, 8)

    class Ring:
        def __init__(self, buf):
            self.buf = buf

        def at(self, v, first, count):
            return self.buf.at[pl.ds(pl.multiple_of(v * CB + c * RB + first * QB, 16), count * QB)]

        def both(self, up, down):
            pair = []
            for (v, first, count), peer in ((up, to_xp), (down, to_xm)):
                ref = self.at(v, first, count)
                pair.append(cp.start(ref, ref, peer))
            return pair

        def share(self, waits, blocks):
            made = []
            for wait, (v, first, count) in zip(waits, blocks):
                wait.wait_recv()
                ref = self.at(v, first, count)
                made.append(cp.start(ref, ref, to_pair))
            return made

        def oa(self):
            self.a = self.both((x, 0, 1), (x, 2, 1))

        def ob(self):
            self.b = self.both((x, 1, 1), (x, 3, 1))
            whole = self.at(x, 0, 4)
            self.d0 = cp.start(whole, whole, to_pair)

        def oc(self):
            self.c = self.both((x, 2, 2), (x, 0, 2))

        def relay(self, waits, up, down):
            pair = []
            for wait, (v, first, count), peer in zip(waits, (up, down), (to_xp, to_xm)):
                wait.wait_recv()
                ref = self.at(v, first, count)
                pair.append(cp.start(ref, ref, peer))
                self.near.append(cp.start(ref, ref, to_pair))
            return pair

        def ra(self):
            self.near = []
            self.ra_made = self.relay(self.a, (xm, 0, 1), (xp, 2, 1))

        def rb(self):
            self.rb_made = self.relay(self.b, (xm, 1, 1), (xp, 3, 1))

        def nr(self):
            self.near += self.share(self.c, ((xm, 2, 2), (xp, 0, 2)))

        def nw(self):
            for made in self.near:
                made.wait_recv()

        def fa(self):
            self.far = self.share(self.ra_made, ((xf, 0, 1), (xf, 2, 1)))

        def fb(self):
            self.far += self.share(self.rb_made, ((xf, 1, 1), (xf, 3, 1)))

        def fw(self):
            for made in self.far:
                made.wait_recv()

    class Weights:
        def __init__(self, buf):
            self.buf, self.deep = buf, buf.shape[3]

        def s0(self):
            half = self.deep // 2
            parts = pl.ds(0, half), pl.ds(half, half)
            self.first = []
            for turn in range(2):
                lo, hi = parts[turn], parts[1 - turn]
                plan = (
                    (self.buf.at[0, z, y, lo], to_yp),
                    (self.buf.at[1, z, y, lo], to_zp),
                    (self.buf.at[0, z, y, hi], to_ym),
                    (self.buf.at[1, z, y, hi], to_zm),
                )
                self.first += [cp.start(ref, ref, peer) for ref, peer in plan]

        def s1(self):
            half = self.deep // 2
            lo, hi = pl.ds(0, half), pl.ds(half, half)
            plan = (
                (self.buf.at[0, z, ym, lo], to_yp),
                (self.buf.at[1, zm, y, lo], to_zp),
                (self.buf.at[0, z, yp, hi], to_ym),
                (self.buf.at[1, zp, y, hi], to_zm),
            )
            self.second = []
            for made, (ref, peer) in zip(self.first, plan):
                made.wait_recv()
                self.second.append(cp.start(ref, ref, peer))

        def s2(self):
            for made in self.first[4:] + self.second:
                made.wait_recv()
            parts = pl.ds(0, 2), pl.ds(2, 2)
            self.third = []
            for turn in range(2):
                lo, hi = parts[turn], parts[1 - turn]
                plan = (
                    (self.buf.at[0, z, lo], to_zp),
                    (self.buf.at[1, lo, y], to_yp),
                    (self.buf.at[0, z, hi], to_zm),
                    (self.buf.at[1, hi, y], to_ym),
                )
                self.third += [cp.start(ref, ref, peer) for ref, peer in plan]

        def s3(self):
            lo, hi = pl.ds(0, 2), pl.ds(2, 2)
            plan = (
                (self.buf.at[0, zm, lo], to_zp),
                (self.buf.at[1, lo, ym], to_yp),
                (self.buf.at[0, zp, hi], to_zm),
                (self.buf.at[1, hi, yp], to_ym),
            )
            self.fourth = []
            for made, (ref, peer) in zip(self.third, plan):
                made.wait_recv()
                self.fourth.append(cp.start(ref, ref, peer))

        def s4(self):
            for made in self.third[4:] + self.fourth:
                made.wait_recv()

    ring1, ring2 = Ring(x1), Ring(x2)
    gv, gp, gu, gd = Weights(vg), Weights(pp), Weights(uu), Weights(dd)

    def point_rows(v, first, count):
        rows = pl.ds(pl.multiple_of((v % 2) * 256 + first, 128), count)
        return pp.at[v // 2, z, y, rows]

    steps = {}
    made = {}

    def step_named(name):
        def keep(body):
            steps[name] = body
            return body

        return keep

    for name, chain in (("V", gv), ("P", gp), ("U", gu), ("D", gd)):
        for part in ("s0", "s1", "s2", "s3", "s4"):
            steps[name + "." + part] = getattr(chain, part)
    for name, chain in (("R1", ring1), ("R2", ring2)):
        for part in ("oa", "ob", "oc", "ra", "rb", "nr", "nw", "fa", "fb", "fw"):
            steps[name + "." + part] = getattr(chain, part)

    def wait(*names):
        for name in names:
            made[name].wait_recv()

    def send_point(name, v, first, count, peer):
        ref = pp.at[v // 2, z, y, pl.ds(pl.multiple_of((v % 2) * 256 + first, 128), count)]
        made[name] = cp.start(ref, ref, peer)

    @step_named("px.0")
    def _():
        send_point("pxp", x, 0, 256, to_xp)
        send_point("pxm", x, 0, 256, to_xm)

    @step_named("px.1")
    def _():
        wait("pxp")
        send_point("pxl", xm, 0, 128, to_xp)
        wait("pxm")
        send_point("pxh", xp, 128, 128, to_xm)

    steps["px.2"] = lambda: wait("pxl", "pxh")

    @step_named("c.init")
    def _():
        glu[0:HALO, :] = jnp.zeros((HALO, CW), BF)
        glu[HALO + SEQ : HALO + SEQ + HALO, :] = jnp.zeros((HALO, CW), BF)
        st[...] = jnp.zeros(st.shape, F32)

    own_cols = pl.ds(pl.multiple_of(tp * CW, CW), CW)

    def gated(v):
        rows = pl.multiple_of(v * CB, CB)
        block = x1[pl.ds(rows, CB), :]
        value = dot(block, vg[0].reshape(D, CW)) * value_scale[:, own_cols]
        gate = dot(block, vg[1].reshape(D, CW)) * gate_scale[:, own_cols]
        glu[pl.ds(pl.multiple_of(rows + HALO, 16), CB), :] = (value * jax.nn.sigmoid(gate)).astype(BF)

    @step_named("c.gx")
    def _():
        ring1.d0.wait_recv()
        gated(x)

    steps["c.gp"] = lambda: gated(xp)

    def send_glu(name, v, first, count, peer):
        rows = pl.ds(pl.multiple_of(v * CB + first, 16), count)
        made[name] = cp.start(glu.at[rows], cin.at[x, pl.ds(first, count)], peer)

    def send_far(name, first, slot, peer):
        rows = pl.ds(pl.multiple_of(xf * CB + first, 16), FAR)
        made[name] = cp.start(glu.at[rows], far_in.at[slot], peer)

    steps["c.sp"] = lambda: send_glu("gp", xp, 0, CB + HALO, to_xp)

    @step_named("c.gm")
    def _():
        gated(xm)
        send_glu("gm", xm, HALO, CB + HALO, to_xm)

    @step_named("c.gf")
    def _():
        gated(xf)
        send_far("fl", 0, 0, to_xp)
        send_far("fh", FAR, 1, to_xm)
        send_glu("ep", xp, CB + HALO, HALO, to_xp)
        send_glu("em", xm, 0, HALO, to_xm)

    def convolve(v):
        def step(i, carry):
            part, chunk = i % 2, i // 2
            lane = pl.multiple_of(part * 128, 128)
            row = pl.multiple_of(chunk * 64, 64)
            col = pl.multiple_of((2 * v + c) * CW + part * 128, 128)
            data = cin[v, pl.ds(row, 96), pl.ds(lane, 128)].astype(F32)
            total = jnp.zeros((64, 128), F32)
            for b in range(8):
                turned = data if b == 0 else pltpu.roll(data, 96 - b, 0)
                for a in range(4):
                    k = 8 * a + b
                    if k:
                        tap = taps[k - 1 : k, pl.ds(col, 128)]
                        total = total + tap * turned[8 * a : 8 * a + 64]
            cv[v, pl.ds(row, 64), pl.ds(lane, 128)] = total
            st[0, pl.ds(row, 64), :] += total
            st[1, pl.ds(row, 64), :] += total * total
            return carry

        lax.fori_loop(0, 12, step, 0)

    @step_named("c.cx")
    def _():
        cin[x] = glu[pl.ds(pl.multiple_of(x * CB, CB), CB + 2 * HALO), :]
        convolve(x)

    @step_named("c.fr")
    def _():
        wait("fl")
        made["l2"] = cp.start(far_in.at[0], cin.at[xm, pl.ds(0, FAR)], to_xp)
        wait("fh")
        made["h2"] = cp.start(far_in.at[1], cin.at[xp, pl.ds(FAR, FAR)], to_xm)

    @step_named("c.cm")
    def _():
        wait("gp", "ep")
        convolve(xm)

    @step_named("c.cp")
    def _():
        wait("gm", "em")
        convolve(xp)

    @step_named("c.cf")
    def _():
        wait("l2", "h2")
        convolve(xf)

    @step_named("c.st")
    def _():
        for kind in range(2):
            total = st[kind]
            for shift in (4, 8, 16, 32, 64):
                total = total + pltpu.roll(total, shift, 1)
            st[kind] = total
        made["st"] = cp.start(st, st_in, to_pair)

    def activate(i, carry):
        rows = pl.ds(pl.multiple_of(i * 32, 32), 32)
        gmean = (st[0, rows, :] + st_in[0, rows, :]) / GROUP_WIDTH
        gsquare = (st[1, rows, :] + st_in[1, rows, :]) / GROUP_WIDTH
        inv = lax.rsqrt(gsquare - gmean * gmean + 1e-05)
        for v in range(4):
            for part in range(2):
                col = pl.multiple_of((2 * v + c) * CW + part * 128, 128)
                lane = part * 128
                s = (cv[v, rows, lane : lane + 128] - gmean) * inv * conv_gain[:, pl.ds(col, 128)]
                act[rows, v * CW + lane : v * CW + lane + 128] = (s / (1.0 + jnp.exp(-s))).astype(BF)
        return carry

    @step_named("c.ac")
    def _():
        wait("st")
        lax.fori_loop(0, CB // 32, activate, 0)

    pair_rows = pl.ds(pl.multiple_of((1 - c) * RB, RB), RB)
    own_rows = pl.ds(pl.multiple_of(c * RB, RB), RB)
    mix_at = cp.take(8)

    def mix_copy(n):
        return cp.copy(mix_out.at[n], mix_in.at[n], to_pair, mix_at + n)

    def columns(buf, half, n):
        two = buf[half, n // 2, pl.ds((n % 2) * 2, 2)]
        return jnp.concatenate([two[0], two[1]], axis=1)

    def point(n, carry):
        left = jnp.concatenate([act[pair_rows, 0:512], act[own_rows, 0:512]], axis=0)
        right = jnp.concatenate([act[pair_rows, 512:1024], act[own_rows, 512:1024]], axis=0)
        both = dot(left, columns(pp, 0, n)) + dot(right, columns(pp, 1, n))
        mix_out[n] = both[:RB].astype(BF)
        mix_copy(n).start()
        mix[:, pl.ds(pl.multiple_of(n * 256, 256), 256)] = both[RB:]
        return carry

    steps["c.pt"] = lambda: lax.fori_loop(0, 8, point, 0)

    def add_mixed(n, carry):
        mix_copy(n).wait_recv()
        cols = pl.ds(pl.multiple_of(n * 256, 256), 256)
        mixed = mix[:, cols] + mix_in[n].astype(F32)
        mid[:, cols] = (resid[:, cols].astype(F32) + mixed).astype(BF)
        return carry

    @step_named("c.nm")
    def _():
        lax.fori_loop(0, 8, add_mixed, 0)
        norm_rows(mid, gain2, x2, tp * RB)

    def up(v):
        rows = pl.ds(pl.multiple_of(v * CB, CB), CB)

        def step(n, carry):
            weight = uu[n // 2, :, :, :, pl.ds(pl.multiple_of((n % 2) * 256, 256), 256)].reshape(D, 256)
            cols = pl.ds(pl.multiple_of(n * 256, 256), 256)
            upper = jnp.maximum(dot(x2[rows, :], weight) * up_scale[:, cols], 0.0)
            hid[rows, cols] = (upper * upper).astype(BF)
            return carry

        lax.fori_loop(0, 4, step, 0)

    @step_named("c.ux")
    def _():
        ring2.d0.wait_recv()
        up(x)

    steps["c.up"] = lambda: up(xp)
    steps["c.um"] = lambda: up(xm)
    steps["c.uf"] = lambda: up(xf)

    pair_at, last_at, out_at = cp.take(32), cp.take(24), cp.take(8)

    def to_other(v, n):
        return cp.copy(par_out.at[v, n], par_in.at[v, n], to_pair, pair_at + v * 8 + n)

    def down(v, n):
        pair_rows = pl.ds(pl.multiple_of(v * CB + (1 - c) * RB, RB), RB)
        own_rows = pl.ds(pl.multiple_of(v * CB + c * RB, RB), RB)
        left = jnp.concatenate([hid[pair_rows, 0:512], hid[own_rows, 0:512]], axis=0)
        right = jnp.concatenate([hid[pair_rows, 512:1024], hid[own_rows, 512:1024]], axis=0)
        both = dot(left, columns(dd, 0, n)) + dot(right, columns(dd, 1, n))
        par_out[v, n] = both[:RB].astype(BF)
        to_other(v, n).start()
        par[v, n] = both[RB:].astype(BF)

    def add_pair(v, n):
        to_other(v, n).wait_recv()
        par[v, n] = (par[v, n].astype(F32) + par_in[v, n].astype(F32)).astype(BF)

    def relay(side, k):
        n = k + 4 * side
        return cp.copy(par.at[xf, n], rel_in.at[side, k], to_xm if side else to_xp, last_at + n)

    def plain(side, k):
        n = k + 4 * (1 - side)
        to, peer = (xm, to_xm) if side else (xp, to_xp)
        return cp.copy(par.at[to, n], fin_in.at[side, n], peer, last_at + 8 + side * 4 + k)

    def last(side, k):
        n = k + 4 * side
        to, peer = (xm, to_xm) if side else (xp, to_xp)
        return cp.copy(par.at[to, n], fin_in.at[side, n], peer, last_at + 16 + side * 4 + k)

    def each(count, body):
        def step(i, carry):
            body(i)
            return carry

        lax.fori_loop(0, count, step, 0)

    def relay_chunk(j):
        add_pair(xf, (j % 2) * 4 + j // 2)

        @pl.when(j % 2 == 0)
        def _():
            relay(0, j // 2).start()

        @pl.when(j % 2 == 1)
        def _():
            relay(1, j // 2).start()

    @step_named("d.fa")
    def _():
        def far_step(i):
            down(xf, (i % 2) * 4 + i // 2)

            @pl.when(i >= 3)
            def _():
                relay_chunk(i - 3)

        each(8, far_step)
        each(3, lambda i: relay_chunk(i + 5))

    @step_named("d.pl")
    def _():
        def plain_chunk(k):
            add_pair(xp, k + 4)
            plain(0, k).start()
            add_pair(xm, k)
            plain(1, k).start()

        def near_step(k):
            down(xp, k + 4)
            down(xm, k)

            @pl.when(k >= 1)
            def _():
                plain_chunk(k - 1)

        each(4, near_step)
        plain_chunk(3)

    @step_named("d.la")
    def _():
        def last_step(k):
            down(xp, k)
            down(xm, k + 4)

        each(4, last_step)

    @step_named("d.sl")
    def _():
        def send_last(k):
            for side, v in ((0, xp), (1, xm)):
                n = k + 4 * side
                to_other(v, n).wait_recv()
                relay(side, k).wait_recv()
                total = par[v, n].astype(F32) + par_in[v, n].astype(F32) + rel_in[side, k].astype(F32)
                par[v, n] = total.astype(BF)
                last(side, k).start()

        each(4, send_last)

    @step_named("d.xx")
    def _():
        each(8, lambda n: down(x, n))

        def own_step(n):
            to_other(x, n).wait_recv()
            cols = pl.ds(pl.multiple_of(n * 256, 256), 256)
            mix[:, cols] = mid[:, cols].astype(F32) + (par[x, n].astype(F32) + par_in[x, n].astype(F32))

        each(8, own_step)

    def out_copy(n):
        cols = pl.ds(pl.multiple_of(n * 256, 256), 256)
        return pltpu.make_async_copy(out_buf.at[n], out.at[:, cols], recv_sem.at[out_at + n])

    def finish(k):
        for n, near, far in ((k, last(0, k), plain(1, k)), (k + 4, plain(0, k), last(1, k))):
            near.wait_recv()
            far.wait_recv()
            cols = pl.ds(pl.multiple_of(n * 256, 256), 256)
            total = fin_in[0, n].astype(F32) + fin_in[1, n].astype(F32)
            out_buf[n] = (mix[:, cols] + total).astype(BF)
            out_copy(n).start()

    steps["d.fn"] = lambda: each(4, finish)
    for name in ORDER:
        with jax.named_scope(name):
            steps[name]()
    assert len(ORDER) == len(set(ORDER)) == len(steps)
    cp.finish()

    def sent(n):
        mix_copy(n).wait_send()
        for v in range(4):
            to_other(v, n).wait_send()
        out_copy(n).wait()

    each(8, sent)

    def sent_last(k):
        for side in range(2):
            for made in (relay(side, k), plain(side, k), last(side, k)):
                made.wait_send()

    each(4, sent_last)


SCRATCH = (
    ((SEQ, D), BF),
    ((SEQ, D), BF),
    ((2, 4, 4, 128, 256), BF),
    ((2, 4, 4, 512, 128), BF),
    ((2, 4, 4, 128, 512), BF),
    ((2, 4, 4, 512, 128), BF),
    ((SEQ + 2 * HALO, CW), BF),
    ((4, CB + 2 * HALO, CW), BF),
    ((4, CB, CW), F32),
    ((2, CB, 128), F32),
    ((2, CB, 128), F32),
    ((CB, 4 * CW), BF),
    ((8, RB, 256), BF),
    ((8, RB, 256), BF),
    ((RB, D), F32),
    ((RB, D), BF),
    ((SEQ, 1024), BF),
    ((4, 8, RB, 256), BF),
    ((4, 8, RB, 256), BF),
    ((4, 8, RB, 256), BF),
    ((2, 4, RB, 256), BF),
    ((2, 8, RB, 256), BF),
    ((2, FAR, CW), BF),
    ((8, RB, 256), BF),
)


def shards(*arrays):
    flat = [a.reshape(1, -1) if a.ndim == 1 else a for a in arrays]
    return pl.pallas_call(
        kernel,
        out_shape=jax.ShapeDtypeStruct((RB, D), BF),
        in_specs=[pl.BlockSpec(memory_space=pltpu.VMEM)] * len(flat),
        out_specs=pl.BlockSpec(memory_space=pl.ANY),
        scratch_shapes=[pltpu.VMEM(shape, kind) for shape, kind in SCRATCH]
        + [pltpu.SemaphoreType.DMA((N_SEM,)), pltpu.SemaphoreType.DMA((N_SEM,))],
        compiler_params=pltpu.CompilerParams(
            collective_id=0, has_side_effects=True, vmem_limit_bytes=66 * 1000 * 1000
        ),
        name="layer",
    )(*flat)


def solution(mesh):
    in_specs = (
        P(("fs", "tp"), None),
        P(),
        P("fs", "tp"),
        P("fs", "tp"),
        P(),
        P(),
        P(),
        P(),
        P("tp", "fs"),
        P("fs"),
        P(),
        P("fs", "tp"),
        P("tp"),
        P("tp", "fs"),
        P("fs"),
    )
    out_specs = P(("fs", "tp"), None)
    return jax.shard_map(shards, mesh=mesh, in_specs=in_specs, out_specs=out_specs, check_vma=False)
```

time: 140 us -> 125 us (0.89)
  Pallas kernels: 137 us -> 123 us
    pallas_call x1, Pallas kernels: 137 us -> 123 us  [shards(): pl.pallas_call(kernel, out_shape=jax.ShapeDtypeStruct((RB, D), BF), in_sp...]
where the time goes in v2:
time: 125 us
  Pallas kernels  123 us (98%)
  local copies, waits for them, and re-layouts  2.09 us (2%)
    pallas_call x1, Pallas kernels, shards(): pl.pallas_call(kernel, out_shape=jax.ShapeDtypeStruct((RB, D), BF), in_sp...  123 us

profile of v2, /device:TPU:1, one launch (start us, length us, event | category | flops | bytes accessed | tf_op | source)
XLA Modules:
  0.0 124.9 jit_solution(13355883953321608282)
XLA Ops:
  0.0 122.8 %layer.1 = bf16[192,2048]{1,0:T(8,128)(2,1)} custom-call(bf16[192,2048]{1,0:T(8,128)(2,1)} %resid.1, f32[1,2048]{1,0:T(1,128)} %bitcast.8, f32[128,256]{1,0:T(8,128)} %w_value.1, f32[128,256]{1,0:T(8,128)} %w_gate.1, f32[1,2048]{1,0:T(1,128)} %bitcast.9, f32[1,2048]{1,0:T(1,128)} %bitcast.10, f32[31,2048]{1,0:T(8,128)} %taps.1, f32[1,2048]{1,0:T(1,128)} %bitcast.11, ...), custom_call_target="tpu_custom_call" | custom-call | tf_op jit(solution)/shard_map/layer/pallas_call | solution.py:687
  122.8 2.1 %copy.17 = bf16[192,2048]{1,0:T(8,128)(2,1)} copy(bf16[192,2048]{1,0:T(8,128)(2,1)} %layer.1) | data formatting | bytes 1572864

commit v3 on v2

v3 whole, which is shorter than its diff:
```python
import functools

import jax
import jax.numpy as jnp
from jax import lax
from jax.experimental import pallas as pl
from jax.experimental.pallas import tpu as pltpu
from jax.sharding import PartitionSpec as P

BF = jnp.bfloat16
F32 = jnp.float32
MESH = pl.DeviceIdType.MESH

RB = 192
QB = 48
CB = 384
SEQ = 1536
D = 2048
CW = 256
HALO = 16
FAR = 208
KERNEL = 31
GROUP_WIDTH = 512.0
N_SEND, N_RECV = 12, 112

ORDER = (
    "V.s0", "px.0", "c.n1", "R1.oa", "c.ld", "D.s0", "px.1", "V.s1", "R1.ob", "U.s0", "c.init", "V.s2",
    "R1.oc", "U.s1", "px.2", "P.s0", "R1.ra", "V.s3", "R1.rb", "P.s1", "V.s4", "R1.nr", "D.s1", "c.gx",
    "P.s2", "R1.nw", "c.gp", "R1.fa", "c.sp", "c.gm", "R1.fb", "R1.fw", "c.gf", "P.s3", "c.cx", "c.fr",
    "U.s2", "c.cm", "c.cp", "c.cf", "c.st", "P.s4", "c.ac", "c.pt", "c.nm", "R2.oa", "U.s3", "R2.ob", "R2.oc",
    "D.s2", "R2.ra", "D.s3", "U.s4", "c.ux", "R2.rb", "R2.nr", "R2.nw", "c.up", "R2.fa", "c.um", "D.s4",
    "d.pl", "R2.fb", "R2.fw", "c.uf", "d.fa", "d.la", "d.sl", "d.xx", "d.fn",
)


def dot(a, b):
    return jnp.dot(a, b, preferred_element_type=F32)


class Copies:
    def __init__(self, send, recv, peer):
        self.send, self.recv, self.peer = send, recv, peer
        self.sends, self.recvs, self.finals = 0, 0, []

    def take(self, count=1):
        at = self.recvs
        self.recvs += count
        assert self.recvs <= N_RECV
        return at

    def take_send(self, total):
        at = self.sends
        self.sends += 1
        assert self.sends <= N_SEND
        self.finals.append((total, at))
        return at

    def copy(self, src, dst, device, recv, send):
        return pltpu.make_async_remote_copy(
            src_ref=src,
            dst_ref=dst,
            send_sem=self.send.at[send],
            recv_sem=self.recv.at[recv],
            device_id=device,
            device_id_type=MESH,
        )

    def start(self, ref, device, recv, send):
        self.copy(ref, ref, device, recv, send).start()

    def arrived(self, total, recv):
        self.copy(total, total, self.peer, recv, 0).wait_recv()

    def finish(self):
        for total, at in self.finals:
            self.copy(total, total, self.peer, 0, at).wait_send()


def kernel(*refs):
    hbm, out, local, refs = refs[:15], refs[15], refs[16:31], refs[31:]
    x1, x2, vg, pp, uu, dd, glu, cin, cv, st, st_in, act, mix_out, mix_in, mix, mid, hid = refs[:17]
    par_out, par_in, par, rel_in, fin_in, far_in, out_buf, send_sem, recv_sem, load_sem, out_sem = refs[17:]
    resid, gain1, w_value, w_gate, value_scale, gate_scale, taps, conv_gain = local[:8]
    w_point, point_scale, gain2, w_up, up_scale, w_down, down_scale = local[8:]

    fs = lax.axis_index("fs")
    tp = lax.axis_index("tp")
    z, y = fs // 4, fs % 4
    x, c = tp // 2, tp % 2
    xp, xm, xf = (x + 1) % 4, (x + 3) % 4, (x + 2) % 4
    yp, ym = (y + 1) % 4, (y + 3) % 4
    zp, zm = (z + 1) % 4, (z + 3) % 4
    to_xp, to_xm = ({"tp": v * 2 + c} for v in (xp, xm))
    to_pair = {"tp": x * 2 + 1 - c}
    to_yp, to_ym = ({"fs": z * 4 + v} for v in (yp, ym))
    to_zp, to_zm = ({"fs": v * 4 + y} for v in (zp, zm))
    cp = Copies(send_sem, recv_sem, to_pair)

    barrier = pltpu.get_barrier_semaphore()
    for peer in (to_pair, to_xp, to_xm, to_yp, to_ym, to_zp, to_zm):
        pl.semaphore_signal(barrier, inc=1, device_id=peer, device_id_type=MESH)

    loads = [pltpu.make_async_copy(a, b, load_sem.at[i]) for i, (a, b) in enumerate(zip(hbm, local))]
    for i in (2, 3, 8, 9, 0, 1, 13, 14, 11, 4, 5, 6, 7, 10, 12):
        loads[i].start()

    for i in (2, 3, 8, 9):
        loads[i].wait()
    vg[0, z, y] = w_value[...].astype(BF)
    vg[1, z, y] = w_gate[...].astype(BF)
    own_point = pp.at[x // 2, z, y, pl.ds(pl.multiple_of((x % 2) * 256, 256), 256)]
    own_point[...] = (w_point[...] * point_scale[...]).astype(BF)

    def norm_rows(source, gain, target, base):
        def step(i, carry):
            rows = pl.multiple_of(i * 16, 16)
            v = source[pl.ds(rows, 16), :].astype(F32)
            scale = lax.rsqrt(jnp.mean(v * v, axis=-1, keepdims=True) + 1e-06)
            at = pl.multiple_of(base + i * 16, 16)
            target[pl.ds(at, 16), :] = (v * scale * gain[...]).astype(BF)
            return carry

        lax.fori_loop(0, RB // 16, step, 0)

    class Ring:
        def __init__(self, buf):
            self.buf = buf
            self.sem = {name: cp.take() for name in ("a", "b", "c", "d", "ra", "rb", "near", "far")}
            self.send = cp.take_send(buf.at[0 : 28 * QB])

        def at(self, v, first, count):
            return self.buf.at[pl.ds(pl.multiple_of(v * CB + c * RB + first * QB, 16), count * QB)]

        def both(self, name, up, down):
            for (v, first, count), peer in ((up, to_xp), (down, to_xm)):
                cp.start(self.at(v, first, count), peer, self.sem[name], self.send)

        def share(self, name, *blocks):
            for v, first, count in blocks:
                cp.start(self.at(v, first, count), to_pair, self.sem[name], self.send)

        def arrived(self, name, quarters):
            cp.arrived(self.buf.at[0 : quarters * QB], self.sem[name])

        def oa(self):
            self.both("a", (x, 0, 1), (x, 2, 1))

        def ob(self):
            self.both("b", (x, 1, 1), (x, 3, 1))
            self.share("d", (x, 0, 4))

        def oc(self):
            self.both("c", (x, 2, 2), (x, 0, 2))

        def ra(self):
            self.arrived("a", 2)
            self.both("ra", (xm, 0, 1), (xp, 2, 1))
            self.share("near", (xm, 0, 1), (xp, 2, 1))

        def rb(self):
            self.arrived("b", 2)
            self.both("rb", (xm, 1, 1), (xp, 3, 1))
            self.share("near", (xm, 1, 1), (xp, 3, 1))

        def nr(self):
            self.arrived("c", 4)
            self.share("near", (xm, 2, 2), (xp, 0, 2))

        def nw(self):
            self.arrived("near", 8)

        def fa(self):
            self.arrived("ra", 2)
            self.share("far", (xf, 0, 1), (xf, 2, 1))

        def fb(self):
            self.arrived("rb", 2)
            self.share("far", (xf, 1, 1), (xf, 3, 1))

        def fw(self):
            self.arrived("far", 4)

        def own_wait(self):
            self.arrived("d", 4)

    class Weights:
        def __init__(self, buf):
            self.buf, self.deep = buf, buf.shape[3]
            self.sem = [cp.take() for _ in range(6)]
            rows = 30 * buf.shape[3] * buf.shape[4] // D
            self.send = cp.take_send(x1.at[0:rows])

        def four(self, sem, plan):
            for ref, peer in plan:
                cp.start(ref, peer, self.sem[sem], self.send)

        def s0(self):
            half = self.deep // 2
            parts = pl.ds(0, half), pl.ds(half, half)
            for turn in range(2):
                lo, hi = parts[turn], parts[1 - turn]
                plan = (
                    (self.buf.at[0, z, y, lo], to_yp),
                    (self.buf.at[1, z, y, lo], to_zp),
                    (self.buf.at[0, z, y, hi], to_ym),
                    (self.buf.at[1, z, y, hi], to_zm),
                )
                self.four(turn, plan)

        def s1(self):
            half = self.deep // 2
            lo, hi = pl.ds(0, half), pl.ds(half, half)
            plan = (
                (self.buf.at[0, z, ym, lo], to_yp),
                (self.buf.at[1, zm, y, lo], to_zp),
                (self.buf.at[0, z, yp, hi], to_ym),
                (self.buf.at[1, zp, y, hi], to_zm),
            )
            cp.arrived(self.buf.at[0, 0, 0:2], self.sem[0])
            self.four(2, plan)

        def s2(self):
            cp.arrived(self.buf.at[0, 0, 0:2], self.sem[1])
            cp.arrived(self.buf.at[0, 0, 0:2], self.sem[2])
            parts = pl.ds(0, 2), pl.ds(2, 2)
            for turn in range(2):
                lo, hi = parts[turn], parts[1 - turn]
                plan = (
                    (self.buf.at[0, z, lo], to_zp),
                    (self.buf.at[1, lo, y], to_yp),
                    (self.buf.at[0, z, hi], to_zm),
                    (self.buf.at[1, hi, y], to_ym),
                )
                self.four(3 + turn, plan)

        def s3(self):
            lo, hi = pl.ds(0, 2), pl.ds(2, 2)
            plan = (
                (self.buf.at[0, zm, lo], to_zp),
                (self.buf.at[1, lo, ym], to_yp),
                (self.buf.at[0, zp, hi], to_zm),
                (self.buf.at[1, hi, yp], to_ym),
            )
            cp.arrived(self.buf.at[0, 0:2], self.sem[3])
            self.four(5, plan)

        def s4(self):
            cp.arrived(self.buf.at[0, 0:2], self.sem[4])
            cp.arrived(self.buf.at[0, 0:2], self.sem[5])

    ring1, ring2 = Ring(x1), Ring(x2)
    gv, gp, gu, gd = Weights(vg), Weights(pp), Weights(uu), Weights(dd)

    steps = {}

    def step_named(name):
        def keep(body):
            steps[name] = body
            return body

        return keep

    for name, chain in (("V", gv), ("P", gp), ("U", gu), ("D", gd)):
        for part in ("s0", "s1", "s2", "s3", "s4"):
            steps[name + "." + part] = getattr(chain, part)
    for name, chain in (("R1", ring1), ("R2", ring2)):
        for part in ("oa", "ob", "oc", "ra", "rb", "nr", "nw", "fa", "fb", "fw"):
            steps[name + "." + part] = getattr(chain, part)

    point_sem, point_send = [cp.take() for _ in range(2)], cp.take_send(x1.at[0:48])

    def send_point(turn, v, first, count, peer):
        ref = pp.at[v // 2, z, y, pl.ds(pl.multiple_of((v % 2) * 256 + first, 128), count)]
        cp.start(ref, peer, point_sem[turn], point_send)

    @step_named("px.0")
    def _():
        send_point(0, x, 0, 256, to_xp)
        send_point(0, x, 0, 256, to_xm)

    @step_named("px.1")
    def _():
        cp.arrived(pp.at[0, 0, 0], point_sem[0])
        send_point(1, xm, 0, 128, to_xp)
        send_point(1, xp, 128, 128, to_xm)

    steps["px.2"] = lambda: cp.arrived(pp.at[0, 0, 0, 0:256], point_sem[1])

    @step_named("c.ld")
    def _():
        for i in (13, 14, 11):
            loads[i].wait()
        for half in range(2):
            uu[half, z, y] = w_up[:, half * 512 : half * 512 + 512].astype(BF)
            dd[half, z, y] = (w_down[half * 512 : half * 512 + 512, :] * down_scale[...]).astype(BF)

    @step_named("c.n1")
    def _():
        loads[0].wait()
        loads[1].wait()
        norm_rows(resid, gain1, x1, tp * RB)

    @step_named("c.init")
    def _():
        glu[0:HALO, :] = jnp.zeros((HALO, CW), BF)
        glu[HALO + SEQ : HALO + SEQ + HALO, :] = jnp.zeros((HALO, CW), BF)
        st[...] = jnp.zeros(st.shape, F32)
        for i in (4, 5, 6, 7, 10, 12):
            loads[i].wait()

    own_cols = pl.ds(pl.multiple_of(tp * CW, CW), CW)

    def gated(v):
        rows = pl.multiple_of(v * CB, CB)
        block = x1[pl.ds(rows, CB), :]
        value = dot(block, vg[0].reshape(D, CW)) * value_scale[:, own_cols]
        gate = dot(block, vg[1].reshape(D, CW)) * gate_scale[:, own_cols]
        glu[pl.ds(pl.multiple_of(rows + HALO, 16), CB), :] = (value * jax.nn.sigmoid(gate)).astype(BF)

    @step_named("c.gx")
    def _():
        ring1.own_wait()
        gated(x)

    steps["c.gp"] = lambda: gated(xp)

    glu_sem = {name: cp.take() for name in ("gp", "gm", "end", "far", "two")}
    glu_send = cp.take_send(x1.at[0:208])

    def send_glu(name, v, first, count, peer):
        rows = pl.ds(pl.multiple_of(v * CB + first, 16), count)
        cp.copy(glu.at[rows], cin.at[x, pl.ds(first, count)], peer, glu_sem[name], glu_send).start()

    def send_far(first, slot, peer):
        rows = pl.ds(pl.multiple_of(xf * CB + first, 16), FAR)
        cp.copy(glu.at[rows], far_in.at[slot], peer, glu_sem["far"], glu_send).start()

    def glu_arrived(name, rows):
        cp.arrived(glu.at[0:rows], glu_sem[name])

    steps["c.sp"] = lambda: send_glu("gp", xp, 0, CB + HALO, to_xp)

    @step_named("c.gm")
    def _():
        gated(xm)
        send_glu("gm", xm, HALO, CB + HALO, to_xm)

    @step_named("c.gf")
    def _():
        gated(xf)
        send_far(0, 0, to_xp)
        send_far(FAR, 1, to_xm)
        send_glu("end", xp, CB + HALO, HALO, to_xp)
        send_glu("end", xm, 0, HALO, to_xm)

    def convolve(v):
        def step(i, carry):
            part, chunk = i % 2, i // 2
            lane = pl.multiple_of(part * 128, 128)
            row = pl.multiple_of(chunk * 64, 64)
            col = pl.multiple_of((2 * v + c) * CW + part * 128, 128)
            data = cin[v, pl.ds(row, 96), pl.ds(lane, 128)].astype(F32)
            total = jnp.zeros((64, 128), F32)
            for b in range(8):
                turned = data if b == 0 else pltpu.roll(data, 96 - b, 0)
                for a in range(4):
                    k = 8 * a + b
                    if k:
                        tap = taps[k - 1 : k, pl.ds(col, 128)]
                        total = total + tap * turned[8 * a : 8 * a + 64]
            cv[v, pl.ds(row, 64), pl.ds(lane, 128)] = total
            st[0, pl.ds(row, 64), :] += total
            st[1, pl.ds(row, 64), :] += total * total
            return carry

        lax.fori_loop(0, 12, step, 0)

    @step_named("c.cx")
    def _():
        cin[x] = glu[pl.ds(pl.multiple_of(x * CB, CB), CB + 2 * HALO), :]
        convolve(x)

    @step_named("c.fr")
    def _():
        glu_arrived("far", 2 * FAR)
        for slot, v, peer in ((0, xm, to_xp), (1, xp, to_xm)):
            there = cin.at[v, pl.ds(slot * FAR, FAR)]
            cp.copy(far_in.at[slot], there, peer, glu_sem["two"], glu_send).start()

    @step_named("c.cm")
    def _():
        glu_arrived("gp", CB + HALO)
        glu_arrived("end", 2 * HALO)
        convolve(xm)

    @step_named("c.cp")
    def _():
        glu_arrived("gm", CB + HALO)
        convolve(xp)

    @step_named("c.cf")
    def _():
        glu_arrived("two", 2 * FAR)
        convolve(xf)

    st_sem, st_send = cp.take(), cp.take_send(st)

    @step_named("c.st")
    def _():
        for kind in range(2):
            total = st[kind]
            for shift in (4, 8, 16, 32, 64):
                total = total + pltpu.roll(total, shift, 1)
            st[kind] = total
        cp.copy(st, st_in, to_pair, st_sem, st_send).start()

    def activate(i, carry):
        rows = pl.ds(pl.multiple_of(i * 32, 32), 32)
        gmean = (st[0, rows, :] + st_in[0, rows, :]) / GROUP_WIDTH
        gsquare = (st[1, rows, :] + st_in[1, rows, :]) / GROUP_WIDTH
        inv = lax.rsqrt(gsquare - gmean * gmean + 1e-05)
        for v in range(4):
            for part in range(2):
                col = pl.multiple_of((2 * v + c) * CW + part * 128, 128)
                lane = part * 128
                s = (cv[v, rows, lane : lane + 128] - gmean) * inv * conv_gain[:, pl.ds(col, 128)]
                act[rows, v * CW + lane : v * CW + lane + 128] = (s / (1.0 + jnp.exp(-s))).astype(BF)
        return carry

    @step_named("c.ac")
    def _():
        cp.arrived(st, st_sem)
        lax.fori_loop(0, CB // 32, activate, 0)

    pair_rows = pl.ds(pl.multiple_of((1 - c) * RB, RB), RB)
    own_rows = pl.ds(pl.multiple_of(c * RB, RB), RB)
    mix_sem, mix_send = cp.take(), cp.take_send(mix_out)

    def columns(buf, n):
        halves = []
        for half in range(2):
            two = buf[half, n // 2, pl.ds((n % 2) * 2, 2)]
            halves.append(jnp.concatenate([two[0], two[1]], axis=1))
        return jnp.concatenate(halves, axis=0)

    def point(n, carry):
        rows = jnp.concatenate([act[pair_rows, :], act[own_rows, :]], axis=0)
        both = dot(rows, columns(pp, n))
        mix_out[n] = both[:RB].astype(BF)
        cp.copy(mix_out.at[n], mix_in.at[n], to_pair, mix_sem, mix_send).start()
        mix[:, pl.ds(pl.multiple_of(n * 256, 256), 256)] = both[RB:]
        return carry

    steps["c.pt"] = lambda: lax.fori_loop(0, 8, point, 0)

    def add_mixed(n, carry):
        cols = pl.ds(pl.multiple_of(n * 256, 256), 256)
        mixed = mix[:, cols] + mix_in[n].astype(F32)
        mid[:, cols] = (resid[:, cols].astype(F32) + mixed).astype(BF)
        return carry

    @step_named("c.nm")
    def _():
        cp.arrived(mix_in, mix_sem)
        lax.fori_loop(0, 8, add_mixed, 0)
        norm_rows(mid, gain2, x2, tp * RB)

    def up(v):
        rows = pl.ds(pl.multiple_of(v * CB, CB), CB)

        def step(n, carry):
            weight = uu[n // 2, :, :, :, pl.ds(pl.multiple_of((n % 2) * 256, 256), 256)].reshape(D, 256)
            cols = pl.ds(pl.multiple_of(n * 256, 256), 256)
            upper = jnp.maximum(dot(x2[rows, :], weight) * up_scale[:, cols], 0.0)
            hid[rows, cols] = (upper * upper).astype(BF)
            return carry

        lax.fori_loop(0, 4, step, 0)

    @step_named("c.ux")
    def _():
        ring2.own_wait()
        up(x)

    steps["c.up"] = lambda: up(xp)
    steps["c.um"] = lambda: up(xm)
    steps["c.uf"] = lambda: up(xf)

    pair_sem = {"f": cp.take(8), "pl": cp.take(4), "la": cp.take(4), "x": cp.take()}
    relay_sem, end_sem = cp.take(4), cp.take(4)
    pair_send, ring_send = cp.take_send(par_out), cp.take_send(par.at[0:3])

    def down(v, n, sem):
        pair_rows = pl.ds(pl.multiple_of(v * CB + (1 - c) * RB, RB), RB)
        own_rows = pl.ds(pl.multiple_of(v * CB + c * RB, RB), RB)
        rows = jnp.concatenate([hid[pair_rows, :], hid[own_rows, :]], axis=0)
        both = dot(rows, columns(dd, n))
        par_out[v, n] = both[:RB].astype(BF)
        cp.copy(par_out.at[v, n], par_in.at[v, n], to_pair, sem, pair_send).start()
        par[v, n] = both[RB:].astype(BF)

    def pair_arrived(sem, count):
        cp.arrived(par_in.at[0, 0:count], sem)

    def add_pair(v, n):
        par[v, n] = (par[v, n].astype(F32) + par_in[v, n].astype(F32)).astype(BF)

    def relay(side, k):
        n = k + 4 * side
        cp.copy(par.at[xf, n], rel_in.at[side, k], to_xm if side else to_xp, relay_sem + k, ring_send).start()

    def plain(side, k):
        n = k + 4 * (1 - side)
        to, peer = (xm, to_xm) if side else (xp, to_xp)
        cp.copy(par.at[to, n], fin_in.at[side, n], peer, end_sem + k, ring_send).start()

    def last(side, k):
        n = k + 4 * side
        to, peer = (xm, to_xm) if side else (xp, to_xp)
        cp.copy(par.at[to, n], fin_in.at[side, n], peer, end_sem + k, ring_send).start()

    def each(count, body):
        def step(i, carry):
            body(i)
            return carry

        lax.fori_loop(0, count, step, 0)

    def relay_chunk(j):
        n = (j % 2) * 4 + j // 2
        pair_arrived(pair_sem["f"] + n, 1)
        add_pair(xf, n)

        @pl.when(j % 2 == 0)
        def _():
            relay(0, j // 2)

        @pl.when(j % 2 == 1)
        def _():
            relay(1, j // 2)

    @step_named("d.fa")
    def _():
        def far_step(i):
            n = (i % 2) * 4 + i // 2
            down(xf, n, pair_sem["f"] + n)

            @pl.when(i >= 3)
            def _():
                relay_chunk(i - 3)

        each(8, far_step)
        each(3, lambda i: relay_chunk(i + 5))

    @step_named("d.pl")
    def _():
        def plain_chunk(k):
            pair_arrived(pair_sem["pl"] + k, 2)
            add_pair(xp, k + 4)
            plain(0, k)
            add_pair(xm, k)
            plain(1, k)

        def near_step(k):
            down(xp, k + 4, pair_sem["pl"] + k)
            down(xm, k, pair_sem["pl"] + k)

            @pl.when(k >= 1)
            def _():
                plain_chunk(k - 1)

        each(4, near_step)
        plain_chunk(3)

    @step_named("d.la")
    def _():
        def last_step(k):
            down(xp, k, pair_sem["la"] + k)
            down(xm, k + 4, pair_sem["la"] + k)

        each(4, last_step)

    @step_named("d.sl")
    def _():
        def send_last(k):
            pair_arrived(pair_sem["la"] + k, 2)
            cp.arrived(rel_in.at[0, 0:2], relay_sem + k)
            for side, v in ((0, xp), (1, xm)):
                n = k + 4 * side
                total = par[v, n].astype(F32) + par_in[v, n].astype(F32) + rel_in[side, k].astype(F32)
                par[v, n] = total.astype(BF)
                last(side, k)

        each(4, send_last)

    @step_named("d.xx")
    def _():
        each(8, lambda n: down(x, n, pair_sem["x"]))
        pair_arrived(pair_sem["x"], 8)

        def own_step(n):
            cols = pl.ds(pl.multiple_of(n * 256, 256), 256)
            mix[:, cols] = mid[:, cols].astype(F32) + (par[x, n].astype(F32) + par_in[x, n].astype(F32))

        each(8, own_step)

    def out_copy(n):
        cols = pl.ds(pl.multiple_of(n * 256, 256), 256)
        return pltpu.make_async_copy(out_buf.at[n], out.at[:, cols], out_sem.at[0])

    def finish(k):
        cp.arrived(fin_in.at[0, 0:4], end_sem + k)
        for n in (k, k + 4):
            cols = pl.ds(pl.multiple_of(n * 256, 256), 256)
            total = fin_in[0, n].astype(F32) + fin_in[1, n].astype(F32)
            out_buf[n] = (mix[:, cols] + total).astype(BF)
            out_copy(n).start()

    steps["d.fn"] = lambda: each(4, finish)
    pl.semaphore_wait(barrier, 7)
    for name in ORDER:
        with jax.named_scope(name):
            steps[name]()
    assert len(ORDER) == len(set(ORDER)) == len(steps)
    cp.finish()
    pltpu.make_async_copy(resid, out, out_sem.at[0]).wait()


SCRATCH = (
    ((SEQ, D), BF),
    ((SEQ, D), BF),
    ((2, 4, 4, 128, 256), BF),
    ((2, 4, 4, 512, 128), BF),
    ((2, 4, 4, 128, 512), BF),
    ((2, 4, 4, 512, 128), BF),
    ((SEQ + 2 * HALO, CW), BF),
    ((4, CB + 2 * HALO, CW), BF),
    ((4, CB, CW), F32),
    ((2, CB, 128), F32),
    ((2, CB, 128), F32),
    ((CB, 4 * CW), BF),
    ((8, RB, 256), BF),
    ((8, RB, 256), BF),
    ((RB, D), F32),
    ((RB, D), BF),
    ((SEQ, 1024), BF),
    ((4, 8, RB, 256), BF),
    ((4, 8, RB, 256), BF),
    ((4, 8, RB, 256), BF),
    ((2, 4, RB, 256), BF),
    ((2, 8, RB, 256), BF),
    ((2, FAR, CW), BF),
    ((8, RB, 256), BF),
)


def shards(*arrays):
    flat = [a.reshape(1, -1) if a.ndim == 1 else a for a in arrays]
    return pl.pallas_call(
        kernel,
        out_shape=jax.ShapeDtypeStruct((RB, D), BF),
        in_specs=[pl.BlockSpec(memory_space=pltpu.HBM)] * len(flat),
        out_specs=pl.BlockSpec(memory_space=pl.ANY),
        scratch_shapes=[pltpu.VMEM(a.shape, a.dtype) for a in flat]
        + [pltpu.VMEM(shape, kind) for shape, kind in SCRATCH]
        + [pltpu.SemaphoreType.DMA((count,)) for count in (N_SEND, N_RECV, len(flat), 1)],
        compiler_params=pltpu.CompilerParams(
            collective_id=0, has_side_effects=True, vmem_limit_bytes=66 * 1000 * 1000
        ),
        name="layer",
    )(*flat)


def solution(mesh):
    in_specs = (
        P(("fs", "tp"), None),
        P(),
        P("fs", "tp"),
        P("fs", "tp"),
        P(),
        P(),
        P(),
        P(),
        P("tp", "fs"),
        P("fs"),
        P(),
        P("fs", "tp"),
        P("tp"),
        P("tp", "fs"),
        P("fs"),
    )
    out_specs = P(("fs", "tp"), None)
    return jax.shard_map(shards, mesh=mesh, in_specs=in_specs, out_specs=out_specs, check_vma=False)
```

time: 125 us -> 119 us (0.952)
  Pallas kernels: 123 us -> 117 us
    pallas_call x1, Pallas kernels: 123 us -> 117 us  [shards(): pl.pallas_call(kernel, out_shape=jax.ShapeDtypeStruct((RB, D), BF), in_sp...]
where the time goes in v3:
time: 119 us
  Pallas kernels  117 us (98%)
  local copies, waits for them, and re-layouts  2.09 us (2%)
    pallas_call x1, Pallas kernels, shards(): pl.pallas_call(kernel, out_shape=jax.ShapeDtypeStruct((RB, D), BF), in_sp...  117 us

profile of v3, /device:TPU:1, one launch (start us, length us, event | category | flops | bytes accessed | tf_op | source)
XLA Modules:
  0.0 119.1 jit_solution(9783035503006392431)
XLA Ops:
  0.0 117.0 %layer.1 = bf16[192,2048]{1,0:T(8,128)(2,1)} custom-call(bf16[192,2048]{1,0:T(8,128)(2,1)} %refs_0_.1, f32[1,2048]{1,0:T(1,128)} %bitcast.8, f32[128,256]{1,0:T(8,128)} %refs_2_.1, f32[128,256]{1,0:T(8,128)} %refs_3_.1, f32[1,2048]{1,0:T(1,128)} %bitcast.9, f32[1,2048]{1,0:T(1,128)} %bitcast.10, f32[31,2048]{1,0:T(8,128)} %refs_6_.1, f32[1,2048]{1,0:T(1,128)} %bitcast.11, ...), custom_call_target="tpu_custom_call" | custom-call | tf_op jit(solution)/shard_map/layer/pallas_call | solution.py:659
  117.0 2.1 %copy.17 = bf16[192,2048]{1,0:T(8,128)(2,1)} copy(bf16[192,2048]{1,0:T(8,128)(2,1)} %layer.1) | data formatting | bytes 1572864

commit v4 on v3

--- a/solution.py
+++ b/solution.py
@@ -21,15 +21,16 @@
 FAR = 208
 KERNEL = 31
 GROUP_WIDTH = 512.0
-N_SEND, N_RECV = 12, 112
+N_SEND, N_RECV = 12, 96
 
 ORDER = (
-    "V.s0", "px.0", "c.n1", "R1.oa", "c.ld", "D.s0", "px.1", "V.s1", "R1.ob", "U.s0", "c.init", "V.s2",
-    "R1.oc", "U.s1", "px.2", "P.s0", "R1.ra", "V.s3", "R1.rb", "P.s1", "V.s4", "R1.nr", "D.s1", "c.gx",
-    "P.s2", "R1.nw", "c.gp", "R1.fa", "c.sp", "c.gm", "R1.fb", "R1.fw", "c.gf", "P.s3", "c.cx", "c.fr",
-    "U.s2", "c.cm", "c.cp", "c.cf", "c.st", "P.s4", "c.ac", "c.pt", "c.nm", "R2.oa", "U.s3", "R2.ob", "R2.oc",
-    "D.s2", "R2.ra", "D.s3", "U.s4", "c.ux", "R2.rb", "R2.nr", "R2.nw", "c.up", "R2.fa", "c.um", "D.s4",
-    "d.pl", "R2.fb", "R2.fw", "c.uf", "d.fa", "d.la", "d.sl", "d.xx", "d.fn",
+    "V.s0", "px.0", "c.n1", "R1.oa", "c.ld", "R1.ob", "D.s0", "px.1", "V.s1", "U.s0", "V.s2", "c.init",
+    "R1.oc", "px.2", "P.s0", "V.s3", "P.s1", "R1.ra", "R1.rb", "V.s4", "R1.nr", "U.s1", "P.s2", "R1.nw",
+    "c.gx", "c.gp", "c.sp", "R1.fa", "c.gm", "D.s1", "R1.fb", "R1.fw", "c.gf", "c.cx", "P.s3", "c.fr", "c.cm",
+    "U.s2", "c.cp", "c.cf", "c.st", "c.a0", "P.s4", "c.p0", "c.m0", "R2.oa", "U.s3", "c.a1", "c.p1", "D.s2",
+    "c.m1", "R2.ob", "R2.ra", "U.s4", "R2.rb", "D.s3", "c.ux", "R2.nr", "R2.nw", "c.up", "c.um", "D.s4",
+    "R2.fa", "d.ep", "D.s5", "d.sp", "R2.fb", "d.pl", "R2.fw", "c.uf", "d.ef", "d.sf", "d.fa", "d.la", "d.sl",
+    "d.xx", "d.fn",
 )
 
 
@@ -111,7 +112,7 @@
     own_point = pp.at[x // 2, z, y, pl.ds(pl.multiple_of((x % 2) * 256, 256), 256)]
     own_point[...] = (w_point[...] * point_scale[...]).astype(BF)
 
-    def norm_rows(source, gain, target, base):
+    def norm_rows(source, gain, target, base, first=0, count=RB // 16):
         def step(i, carry):
             rows = pl.multiple_of(i * 16, 16)
             v = source[pl.ds(rows, 16), :].astype(F32)
@@ -120,7 +121,7 @@
             target[pl.ds(at, 16), :] = (v * scale * gain[...]).astype(BF)
             return carry
 
-        lax.fori_loop(0, RB // 16, step, 0)
+        lax.fori_loop(first, first + count, step, 0)
 
     class Ring:
         def __init__(self, buf):
@@ -182,6 +183,44 @@
 
         def own_wait(self):
             self.arrived("d", 4)
+
+    class LateRing(Ring):
+        def __init__(self, buf):
+            super().__init__(buf)
+            self.rc = cp.take()
+
+        def oa(self):
+            self.both("a", (x, 0, 2), (x, 0, 2))
+
+        def ob(self):
+            self.both("b", (x, 2, 1), (x, 2, 1))
+            self.both("c", (x, 3, 1), (x, 3, 1))
+            self.share("d", (x, 0, 4))
+
+        def ra(self):
+            self.arrived("a", 4)
+            cp.start(self.at(xm, 0, 2), to_xp, self.sem["ra"], self.send)
+            self.share("near", (xm, 0, 2), (xp, 0, 2))
+
+        def rb(self):
+            self.arrived("b", 2)
+            cp.start(self.at(xp, 2, 1), to_xm, self.sem["rb"], self.send)
+            self.share("near", (xm, 2, 1), (xp, 2, 1))
+
+        def nr(self):
+            self.arrived("c", 2)
+            cp.start(self.at(xp, 3, 1), to_xm, self.rc, self.send)
+            self.share("near", (xm, 3, 1), (xp, 3, 1))
+
+        def fa(self):
+            self.arrived("rb", 1)
+            self.share("far", (xf, 2, 1))
+
+        def fb(self):
+            self.arrived("ra", 2)
+            self.share("far", (xf, 0, 2))
+            cp.arrived(self.buf.at[0:QB], self.rc)
+            self.share("far", (xf, 3, 1))
 
     class Weights:
         def __init__(self, buf):
@@ -248,7 +287,7 @@
             cp.arrived(self.buf.at[0, 0:2], self.sem[4])
             cp.arrived(self.buf.at[0, 0:2], self.sem[5])
 
-    ring1, ring2 = Ring(x1), Ring(x2)
+    ring1, ring2 = Ring(x1), LateRing(x2)
     gv, gp, gu, gd = Weights(vg), Weights(pp), Weights(uu), Weights(dd)
 
     steps = {}
@@ -263,8 +302,11 @@
     for name, chain in (("V", gv), ("P", gp), ("U", gu), ("D", gd)):
         for part in ("s0", "s1", "s2", "s3", "s4"):
             steps[name + "." + part] = getattr(chain, part)
+    steps["D.s4"] = lambda: cp.arrived(dd.at[0, 0:2], gd.sem[4])
+    steps["D.s5"] = lambda: cp.arrived(dd.at[0, 0:2], gd.sem[5])
+    steps["R1.oc"] = ring1.oc
     for name, chain in (("R1", ring1), ("R2", ring2)):
-        for part in ("oa", "ob", "oc", "ra", "rb", "nr", "nw", "fa", "fb", "fw"):
+        for part in ("oa", "ob", "ra", "rb", "nr", "nw", "fa", "fb", "fw"):
             steps[name + "." + part] = getattr(chain, part)
 
     point_sem, point_send = [cp.take() for _ in range(2)], cp.take_send(x1.at[0:48])
@@ -415,7 +457,7 @@
         cp.copy(st, st_in, to_pair, st_sem, st_send).start()
 
     def activate(i, carry):
-        rows = pl.ds(pl.multiple_of(i * 32, 32), 32)
+        rows = pl.ds(pl.multiple_of((i // 3) * 96 + (i % 3) * 32, 32), 32)
         gmean = (st[0, rows, :] + st_in[0, rows, :]) / GROUP_WIDTH
         gsquare = (st[1, rows, :] + st_in[1, rows, :]) / GROUP_WIDTH
         inv = lax.rsqrt(gsquare - gmean * gmean + 1e-05)
@@ -427,14 +469,17 @@
                 act[rows, v * CW + lane : v * CW + lane + 128] = (s / (1.0 + jnp.exp(-s))).astype(BF)
         return carry
 
-    @step_named("c.ac")
+    def activate_half(half):
+        lax.fori_loop(3 * half, 3 * half + 3, activate, 0)
+        lax.fori_loop(3 * half + 6, 3 * half + 9, activate, 0)
+
+    @step_named("c.a0")
     def _():
         cp.arrived(st, st_sem)
-        lax.fori_loop(0, CB // 32, activate, 0)
-
-    pair_rows = pl.ds(pl.multiple_of((1 - c) * RB, RB), RB)
-    own_rows = pl.ds(pl.multiple_of(c * RB, RB), RB)
-    mix_sem, mix_send = cp.take(), cp.take_send(mix_out)
+        activate_half(0)
+
+    steps["c.a1"] = lambda: activate_half(1)
+    mix_sem, mix_send = cp.take(2), cp.take_send(mix_out)
 
     def columns(buf, n):
         halves = []
@@ -443,39 +488,47 @@
             halves.append(jnp.concatenate([two[0], two[1]], axis=1))
         return jnp.concatenate(halves, axis=0)
 
-    def point(n, carry):
-        rows = jnp.concatenate([act[pair_rows, :], act[own_rows, :]], axis=0)
-        both = dot(rows, columns(pp, n))
-        mix_out[n] = both[:RB].astype(BF)
-        cp.copy(mix_out.at[n], mix_in.at[n], to_pair, mix_sem, mix_send).start()
-        mix[:, pl.ds(pl.multiple_of(n * 256, 256), 256)] = both[RB:]
-        return carry
-
-    steps["c.pt"] = lambda: lax.fori_loop(0, 8, point, 0)
-
-    def add_mixed(n, carry):
-        cols = pl.ds(pl.multiple_of(n * 256, 256), 256)
-        mixed = mix[:, cols] + mix_in[n].astype(F32)
-        mid[:, cols] = (resid[:, cols].astype(F32) + mixed).astype(BF)
-        return carry
-
-    @step_named("c.nm")
-    def _():
-        cp.arrived(mix_in, mix_sem)
-        lax.fori_loop(0, 8, add_mixed, 0)
-        norm_rows(mid, gain2, x2, tp * RB)
+    def half_rows(core, half):
+        return pl.ds(pl.multiple_of(core * RB + half * 96, 32), 96)
+
+    def point(half):
+        def step(n, carry):
+            rows = jnp.concatenate([act[half_rows(1 - c, half), :], act[half_rows(c, half), :]], axis=0)
+            weight = jnp.concatenate([columns(pp, 2 * n), columns(pp, 2 * n + 1)], axis=1)
+            both = dot(rows, weight)
+            mix_out[half, n] = both[:96].astype(BF)
+            cp.copy(mix_out.at[half, n], mix_in.at[half, n], to_pair, mix_sem + half, mix_send).start()
+            mix[half * 96 : half * 96 + 96, pl.ds(pl.multiple_of(n * 512, 512), 512)] = both[96:]
+            return carry
+
+        lax.fori_loop(0, 4, step, 0)
+
+    def middle(half):
+        def step(n, carry):
+            rows = slice(half * 96, half * 96 + 96)
+            cols = pl.ds(pl.multiple_of(n * 512, 512), 512)
+            mixed = mix[rows, cols] + mix_in[half, n].astype(F32)
+            mid[rows, cols] = (resid[rows, cols].astype(F32) + mixed).astype(BF)
+            return carry
+
+        cp.arrived(mix_in.at[half], mix_sem + half)
+        lax.fori_loop(0, 4, step, 0)
+        norm_rows(mid, gain2, x2, tp * RB, 6 * half, 6)
+
+    steps["c.p0"], steps["c.p1"] = (lambda: point(0)), (lambda: point(1))
+    steps["c.m0"], steps["c.m1"] = (lambda: middle(0)), (lambda: middle(1))
 
     def up(v):
         rows = pl.ds(pl.multiple_of(v * CB, CB), CB)
 
         def step(n, carry):
-            weight = uu[n // 2, :, :, :, pl.ds(pl.multiple_of((n % 2) * 256, 256), 256)].reshape(D, 256)
-            cols = pl.ds(pl.multiple_of(n * 256, 256), 256)
+            weight = uu[n].reshape(D, 512)
+            cols = pl.ds(pl.multiple_of(n * 512, 512), 512)
             upper = jnp.maximum(dot(x2[rows, :], weight) * up_scale[:, cols], 0.0)
             hid[rows, cols] = (upper * upper).astype(BF)
             return carry
 
-        lax.fori_loop(0, 4, step, 0)
+        lax.fori_loop(0, 2, step, 0)
 
     @step_named("c.ux")
     def _():
@@ -490,14 +543,23 @@
     relay_sem, end_sem = cp.take(4), cp.take(4)
     pair_send, ring_send = cp.take_send(par_out), cp.take_send(par.at[0:3])
 
-    def down(v, n, sem):
-        pair_rows = pl.ds(pl.multiple_of(v * CB + (1 - c) * RB, RB), RB)
-        own_rows = pl.ds(pl.multiple_of(v * CB + c * RB, RB), RB)
-        rows = jnp.concatenate([hid[pair_rows, :], hid[own_rows, :]], axis=0)
-        both = dot(rows, columns(dd, n))
-        par_out[v, n] = both[:RB].astype(BF)
-        cp.copy(par_out.at[v, n], par_in.at[v, n], to_pair, sem, pair_send).start()
-        par[v, n] = both[RB:].astype(BF)
+    def place(i):
+        dz = (i % 4 + 3 * (i // 4)) % 4
+        turn = (dz // 2 + i // 4) % 2
+        return ((z + dz) % 4) * 2 + (y // 2 + turn) % 2
+
+    def down(*chunks):
+        done = []
+        for v, i, _ in chunks:
+            pair_rows = pl.ds(pl.multiple_of(v * CB + (1 - c) * RB, RB), RB)
+            own_rows = pl.ds(pl.multiple_of(v * CB + c * RB, RB), RB)
+            rows = jnp.concatenate([hid[pair_rows, :], hid[own_rows, :]], axis=0)
+            done.append(dot(rows, columns(dd, place(i))))
+        for (v, i, _), both in zip(chunks, done):
+            par_out[v, i] = both[:RB].astype(BF)
+            par[v, i] = both[RB:].astype(BF)
+        for v, i, sem in chunks:
+            cp.copy(par_out.at[v, i], par_in.at[v, i], to_pair, sem, pair_send).start()
 
     def pair_arrived(sem, count):
         cp.arrived(par_in.at[0, 0:count], sem)
@@ -526,59 +588,67 @@
 
         lax.fori_loop(0, count, step, 0)
 
-    def relay_chunk(j):
-        n = (j % 2) * 4 + j // 2
+    def relay_chunk(side, k):
+        n = side * 4 + k
         pair_arrived(pair_sem["f"] + n, 1)
         add_pair(xf, n)
-
-        @pl.when(j % 2 == 0)
-        def _():
-            relay(0, j // 2)
-
-        @pl.when(j % 2 == 1)
-        def _():
-            relay(1, j // 2)
+        relay(side, k)
+
+    def plain_chunk(k):
+        pair_arrived(pair_sem["pl"] + k, 2)
+        add_pair(xp, k + 4)
+        plain(0, k)
+        add_pair(xm, k)
+        plain(1, k)
+
+    def far_two(k):
+        down((xf, k, pair_sem["f"] + k), (xf, k + 4, pair_sem["f"] + k + 4))
+
+    def near_two(k):
+        down((xp, k + 4, pair_sem["pl"] + k), (xm, k, pair_sem["pl"] + k))
+
+    steps["d.ep"] = lambda: near_two(0)
+
+    @step_named("d.ef")
+    def _():
+        far_two(0)
+        down((xf, 1, pair_sem["f"] + 1))
+
+    steps["d.sp"] = lambda: plain_chunk(0)
+
+    @step_named("d.sf")
+    def _():
+        relay_chunk(0, 0)
+        relay_chunk(1, 0)
+        relay_chunk(0, 1)
 
     @step_named("d.fa")
     def _():
-        def far_step(i):
-            n = (i % 2) * 4 + i // 2
-            down(xf, n, pair_sem["f"] + n)
-
-            @pl.when(i >= 3)
-            def _():
-                relay_chunk(i - 3)
-
-        each(8, far_step)
-        each(3, lambda i: relay_chunk(i + 5))
+        down((xf, 5, pair_sem["f"] + 5), (xf, 2, pair_sem["f"] + 2))
+
+        down((xf, 6, pair_sem["f"] + 6), (xf, 3, pair_sem["f"] + 3))
+        relay_chunk(1, 1)
+        relay_chunk(0, 2)
+        down((xf, 7, pair_sem["f"] + 7))
+        relay_chunk(1, 2)
+        relay_chunk(0, 3)
+        relay_chunk(1, 3)
 
     @step_named("d.pl")
     def _():
-        def plain_chunk(k):
-            pair_arrived(pair_sem["pl"] + k, 2)
-            add_pair(xp, k + 4)
-            plain(0, k)
-            add_pair(xm, k)
-            plain(1, k)
-
         def near_step(k):
-            down(xp, k + 4, pair_sem["pl"] + k)
-            down(xm, k, pair_sem["pl"] + k)
-
-            @pl.when(k >= 1)
+            near_two(k)
+
+            @pl.when(k >= 2)
             def _():
                 plain_chunk(k - 1)
 
-        each(4, near_step)
+        each(3, lambda k: near_step(k + 1))
         plain_chunk(3)
 
     @step_named("d.la")
     def _():
-        def last_step(k):
-            down(xp, k, pair_sem["la"] + k)
-            down(xm, k + 4, pair_sem["la"] + k)
-
-        each(4, last_step)
+        each(4, lambda k: down((xp, k, pair_sem["la"] + k), (xm, k + 4, pair_sem["la"] + k)))
 
     @step_named("d.sl")
     def _():
@@ -595,23 +665,23 @@
 
     @step_named("d.xx")
     def _():
-        each(8, lambda n: down(x, n, pair_sem["x"]))
+        each(4, lambda k: down((x, k, pair_sem["x"]), (x, k + 4, pair_sem["x"])))
         pair_arrived(pair_sem["x"], 8)
 
         def own_step(n):
-            cols = pl.ds(pl.multiple_of(n * 256, 256), 256)
+            cols = pl.ds(pl.multiple_of(place(n) * 256, 256), 256)
             mix[:, cols] = mid[:, cols].astype(F32) + (par[x, n].astype(F32) + par_in[x, n].astype(F32))
 
         each(8, own_step)
 
     def out_copy(n):
-        cols = pl.ds(pl.multiple_of(n * 256, 256), 256)
+        cols = pl.ds(pl.multiple_of(place(n) * 256, 256), 256)
         return pltpu.make_async_copy(out_buf.at[n], out.at[:, cols], out_sem.at[0])
 
     def finish(k):
         cp.arrived(fin_in.at[0, 0:4], end_sem + k)
         for n in (k, k + 4):
-            cols = pl.ds(pl.multiple_of(n * 256, 256), 256)
+            cols = pl.ds(pl.multiple_of(place(n) * 256, 256), 256)
             total = fin_in[0, n].astype(F32) + fin_in[1, n].astype(F32)
             out_buf[n] = (mix[:, cols] + total).astype(BF)
             out_copy(n).start()
@@ -639,8 +709,8 @@
     ((2, CB, 128), F32),
     ((2, CB, 128), F32),
     ((CB, 4 * CW), BF),
-    ((8, RB, 256), BF),
-    ((8, RB, 256), BF),
+    ((2, 4, 96, 512), BF),
+    ((2, 4, 96, 512), BF),
     ((RB, D), F32),
     ((RB, D), BF),
     ((SEQ, 1024), BF),

time: 119 us -> 116 us (0.975)
  Pallas kernels: 117 us -> 113 us
    pallas_call x1, Pallas kernels: 117 us -> 113 us  [shards(): pl.pallas_call(kernel, out_shape=jax.ShapeDtypeStruct((RB, D), BF), in_sp...]
where the time goes in v4:
time: 116 us; the launch traced here: 115 us
  Pallas kernels  113 us (97%)
  local copies, waits for them, and re-layouts  2.09 us (2%)
    pallas_call x1, Pallas kernels, shards(): pl.pallas_call(kernel, out_shape=jax.ShapeDtypeStruct((RB, D), BF), in_sp...  113 us

profile of v4, /device:TPU:1, one launch (start us, length us, event | category | flops | bytes accessed | tf_op | source)
XLA Modules:
  0.0 115.3 jit_solution(6346521237150507252)
XLA Ops:
  0.0 113.3 %layer.1 = bf16[192,2048]{1,0:T(8,128)(2,1)} custom-call(bf16[192,2048]{1,0:T(8,128)(2,1)} %refs_0_.1, f32[1,2048]{1,0:T(1,128)} %bitcast.8, f32[128,256]{1,0:T(8,128)} %refs_2_.1, f32[128,256]{1,0:T(8,128)} %refs_3_.1, f32[1,2048]{1,0:T(1,128)} %bitcast.9, f32[1,2048]{1,0:T(1,128)} %bitcast.10, f32[31,2048]{1,0:T(8,128)} %refs_6_.1, f32[1,2048]{1,0:T(1,128)} %bitcast.11, ...), custom_call_target="tpu_custom_call" | custom-call | tf_op jit(solution)/shard_map/layer/pallas_call | solution.py:729
  113.3 2.1 %copy.17 = bf16[192,2048]{1,0:T(8,128)(2,1)} copy(bf16[192,2048]{1,0:T(8,128)(2,1)} %layer.1) | data formatting | bytes 1572864

commit v5 on v4

--- a/solution.py
+++ b/solution.py
@@ -24,13 +24,25 @@
 N_SEND, N_RECV = 12, 96
 
 ORDER = (
-    "V.s0", "px.0", "c.n1", "R1.oa", "c.ld", "R1.ob", "D.s0", "px.1", "V.s1", "U.s0", "V.s2", "c.init",
-    "R1.oc", "px.2", "P.s0", "V.s3", "P.s1", "R1.ra", "R1.rb", "V.s4", "R1.nr", "U.s1", "P.s2", "R1.nw",
-    "c.gx", "c.gp", "c.sp", "R1.fa", "c.gm", "D.s1", "R1.fb", "R1.fw", "c.gf", "c.cx", "P.s3", "c.fr", "c.cm",
-    "U.s2", "c.cp", "c.cf", "c.st", "c.a0", "P.s4", "c.p0", "c.m0", "R2.oa", "U.s3", "c.a1", "c.p1", "D.s2",
-    "c.m1", "R2.ob", "R2.ra", "U.s4", "R2.rb", "D.s3", "c.ux", "R2.nr", "R2.nw", "c.up", "c.um", "D.s4",
-    "R2.fa", "d.ep", "D.s5", "d.sp", "R2.fb", "d.pl", "R2.fw", "c.uf", "d.ef", "d.sf", "d.fa", "d.la", "d.sl",
-    "d.xx", "d.fn",
+    "c.ld", "V.s0", "px.0", "U.s0", "c.n1", "R1.oa", "px.1", "V.s1", "D.s0", "R1.ob", "V.s2", "px.2", "P.s0",
+    "c.init", "U.s1", "R1.oc", "R1.ra", "R1.rb", "P.s1", "V.s3", "R1.nr", "P.s2", "R1.nw", "R1.fa", "V.s4",
+    "c.gx", "c.gp", "c.sp", "c.gm", "R1.fb", "c.g0", "R1.fw", "c.gf", "c.cx", "P.s3", "D.s1", "c.f0", "c.f1",
+    "c.f2", "c.cm", "U.s2", "c.cp", "c.cf", "c.a0", "P.s4", "c.p0", "c.a1", "c.m0", "R2.oa", "c.p1", "U.s3",
+    "c.m1", "D.s2", "R2.ob", "R2.ra", "U.s4", "c.ux", "R2.rb", "D.s3", "R2.nr", "R2.nw", "c.up", "c.um",
+    "R2.fa", "D.s4", "d.ep", "d.sp", "R2.fb", "R2.fw", "c.uf", "d.ef", "d.sf", "D.s5", "d.pl", "d.fa", "d.la",
+    "d.sl", "d.xx", "d.fn",
+)
+
+
+CHUNKS = (
+    ((0, 0), (0, 1)),
+    ((1, 0), (1, 1)),
+    ((2, 0), (2, 1)),
+    ((2, 2), (2, 3)),
+    ((3, 0), (3, 1)),
+    ((0, 3), (1, 3)),
+    ((0, 2), (1, 2)),
+    ((3, 2), (3, 3)),
 )
 
 
@@ -112,7 +124,7 @@
     own_point = pp.at[x // 2, z, y, pl.ds(pl.multiple_of((x % 2) * 256, 256), 256)]
     own_point[...] = (w_point[...] * point_scale[...]).astype(BF)
 
-    def norm_rows(source, gain, target, base, first=0, count=RB // 16):
+    def norm_rows(source, gain, target, base):
         def step(i, carry):
             rows = pl.multiple_of(i * 16, 16)
             v = source[pl.ds(rows, 16), :].astype(F32)
@@ -121,7 +133,7 @@
             target[pl.ds(at, 16), :] = (v * scale * gain[...]).astype(BF)
             return carry
 
-        lax.fori_loop(first, first + count, step, 0)
+        lax.fori_loop(0, RB // 16, step, 0)
 
     class Ring:
         def __init__(self, buf):
@@ -352,12 +364,15 @@
 
     own_cols = pl.ds(pl.multiple_of(tp * CW, CW), CW)
 
-    def gated(v):
-        rows = pl.multiple_of(v * CB, CB)
-        block = x1[pl.ds(rows, CB), :]
+    def gated_rows(first, count):
+        rows = pl.multiple_of(first, 64)
+        block = x1[pl.ds(rows, count), :]
         value = dot(block, vg[0].reshape(D, CW)) * value_scale[:, own_cols]
         gate = dot(block, vg[1].reshape(D, CW)) * gate_scale[:, own_cols]
-        glu[pl.ds(pl.multiple_of(rows + HALO, 16), CB), :] = (value * jax.nn.sigmoid(gate)).astype(BF)
+        glu[pl.ds(pl.multiple_of(rows + HALO, 16), count), :] = (value * jax.nn.sigmoid(gate)).astype(BF)
+
+    def gated(v):
+        gated_rows(v * CB, CB)
 
     @step_named("c.gx")
     def _():
@@ -366,16 +381,24 @@
 
     steps["c.gp"] = lambda: gated(xp)
 
-    glu_sem = {name: cp.take() for name in ("gp", "gm", "end", "far", "two")}
+    glu_sem = {name: cp.take() for name in ("gp", "gm", "end", "fo", "f1", "f2", "two")}
     glu_send = cp.take_send(x1.at[0:208])
 
     def send_glu(name, v, first, count, peer):
         rows = pl.ds(pl.multiple_of(v * CB + first, 16), count)
         cp.copy(glu.at[rows], cin.at[x, pl.ds(first, count)], peer, glu_sem[name], glu_send).start()
 
-    def send_far(first, slot, peer):
-        rows = pl.ds(pl.multiple_of(xf * CB + first, 16), FAR)
-        cp.copy(glu.at[rows], far_in.at[slot], peer, glu_sem["far"], glu_send).start()
+    def send_far(name, slot, at, count):
+        rows = pl.ds(pl.multiple_of(xf * CB + slot * FAR + at, 16), count)
+        there = far_in.at[slot, pl.ds(at, count)]
+        peer = {"tp": ((x + 1 + 2 * slot) % 4) * 2 + c}
+        cp.copy(glu.at[rows], there, peer, glu_sem[name], glu_send).start()
+
+    def relay_far(name, slot, at, count):
+        glu_arrived(name, count)
+        there = cin.at[(x + 3 + 2 * slot) % 4, pl.ds(pl.multiple_of(slot * FAR + at, 16), count)]
+        peer = {"tp": ((x + 1 + 2 * slot) % 4) * 2 + c}
+        cp.copy(far_in.at[slot, pl.ds(at, count)], there, peer, glu_sem["two"], glu_send).start()
 
     def glu_arrived(name, rows):
         cp.arrived(glu.at[0:rows], glu_sem[name])
@@ -387,47 +410,51 @@
         gated(xm)
         send_glu("gm", xm, HALO, CB + HALO, to_xm)
 
+    @step_named("c.g0")
+    def _():
+        gated_rows(xf * CB + c * RB, RB)
+        send_far("fo", c, 0, FAR)
+
     @step_named("c.gf")
     def _():
-        gated(xf)
-        send_far(0, 0, to_xp)
-        send_far(FAR, 1, to_xm)
+        gated_rows(xf * CB + (1 - c) * RB, RB)
+        send_far("f1", 1 - c, 0, 112)
+        send_far("f2", 1 - c, 112, 96)
         send_glu("end", xp, CB + HALO, HALO, to_xp)
         send_glu("end", xm, 0, HALO, to_xm)
 
-    def convolve(v):
+    def convolve(v, first=0, count=8):
         def step(i, carry):
             part, chunk = i % 2, i // 2
+            half, slot = chunk // 2, chunk % 2
             lane = pl.multiple_of(part * 128, 128)
-            row = pl.multiple_of(chunk * 64, 64)
+            row = pl.multiple_of(slot * RB + half * 96, 32)
             col = pl.multiple_of((2 * v + c) * CW + part * 128, 128)
-            data = cin[v, pl.ds(row, 96), pl.ds(lane, 128)].astype(F32)
-            total = jnp.zeros((64, 128), F32)
+            data = cin[v, pl.ds(row, 128), pl.ds(lane, 128)].astype(F32)
+            total = jnp.zeros((96, 128), F32)
             for b in range(8):
-                turned = data if b == 0 else pltpu.roll(data, 96 - b, 0)
+                turned = data if b == 0 else pltpu.roll(data, 128 - b, 0)
                 for a in range(4):
                     k = 8 * a + b
                     if k:
                         tap = taps[k - 1 : k, pl.ds(col, 128)]
-                        total = total + tap * turned[8 * a : 8 * a + 64]
-            cv[v, pl.ds(row, 64), pl.ds(lane, 128)] = total
-            st[0, pl.ds(row, 64), :] += total
-            st[1, pl.ds(row, 64), :] += total * total
+                        total = total + tap * turned[8 * a : 8 * a + 96]
+            cv[v, pl.ds(row, 96), pl.ds(lane, 128)] = total
+            there = pl.ds(pl.multiple_of(slot * 96, 32), 96)
+            st[half, 0, there, :] += total
+            st[half, 1, there, :] += total * total
             return carry
 
-        lax.fori_loop(0, 12, step, 0)
+        lax.fori_loop(first, first + count, step, 0)
 
     @step_named("c.cx")
     def _():
         cin[x] = glu[pl.ds(pl.multiple_of(x * CB, CB), CB + 2 * HALO), :]
         convolve(x)
 
-    @step_named("c.fr")
-    def _():
-        glu_arrived("far", 2 * FAR)
-        for slot, v, peer in ((0, xm, to_xp), (1, xp, to_xm)):
-            there = cin.at[v, pl.ds(slot * FAR, FAR)]
-            cp.copy(far_in.at[slot], there, peer, glu_sem["two"], glu_send).start()
+    steps["c.f0"] = lambda: relay_far("fo", c, 0, FAR)
+    steps["c.f1"] = lambda: relay_far("f1", 1 - c, 0, 112)
+    steps["c.f2"] = lambda: relay_far("f2", 1 - c, 112, 96)
 
     @step_named("c.cm")
     def _():
@@ -440,26 +467,29 @@
         glu_arrived("gm", CB + HALO)
         convolve(xp)
 
-    @step_named("c.cf")
-    def _():
-        glu_arrived("two", 2 * FAR)
-        convolve(xf)
-
-    st_sem, st_send = cp.take(), cp.take_send(st)
-
-    @step_named("c.st")
-    def _():
+    st_sem, st_send = cp.take(2), cp.take_send(st)
+
+    def finish_stats(half):
         for kind in range(2):
-            total = st[kind]
+            total = st[half, kind]
             for shift in (4, 8, 16, 32, 64):
                 total = total + pltpu.roll(total, shift, 1)
-            st[kind] = total
-        cp.copy(st, st_in, to_pair, st_sem, st_send).start()
+            st[half, kind] = total
+        cp.copy(st.at[half], st_in.at[half], to_pair, st_sem + half, st_send).start()
+
+    @step_named("c.cf")
+    def _():
+        glu_arrived("two", 2 * FAR)
+        for half in range(2):
+            convolve(xf, 4 * half, 4)
+            finish_stats(half)
 
     def activate(i, carry):
         rows = pl.ds(pl.multiple_of((i // 3) * 96 + (i % 3) * 32, 32), 32)
-        gmean = (st[0, rows, :] + st_in[0, rows, :]) / GROUP_WIDTH
-        gsquare = (st[1, rows, :] + st_in[1, rows, :]) / GROUP_WIDTH
+        half = (i // 3) % 2
+        there = pl.ds(pl.multiple_of((i // 6) * 96 + (i % 3) * 32, 32), 32)
+        gmean = (st[half, 0, there, :] + st_in[half, 0, there, :]) / GROUP_WIDTH
+        gsquare = (st[half, 1, there, :] + st_in[half, 1, there, :]) / GROUP_WIDTH
         inv = lax.rsqrt(gsquare - gmean * gmean + 1e-05)
         for v in range(4):
             for part in range(2):
@@ -475,10 +505,14 @@
 
     @step_named("c.a0")
     def _():
-        cp.arrived(st, st_sem)
+        cp.arrived(st.at[0], st_sem)
         activate_half(0)
 
-    steps["c.a1"] = lambda: activate_half(1)
+    @step_named("c.a1")
+    def _():
+        cp.arrived(st.at[1], st_sem + 1)
+        activate_half(1)
+
     mix_sem, mix_send = cp.take(2), cp.take_send(mix_out)
 
     def columns(buf, n):
@@ -504,16 +538,20 @@
         lax.fori_loop(0, 4, step, 0)
 
     def middle(half):
-        def step(n, carry):
-            rows = slice(half * 96, half * 96 + 96)
-            cols = pl.ds(pl.multiple_of(n * 512, 512), 512)
-            mixed = mix[rows, cols] + mix_in[half, n].astype(F32)
-            mid[rows, cols] = (resid[rows, cols].astype(F32) + mixed).astype(BF)
+        def step(i, carry):
+            here = pl.ds(pl.multiple_of(i * 16, 16), 16)
+            rows = pl.ds(pl.multiple_of(half * 96 + i * 16, 16), 16)
+            mixed = mix[rows, :] + jnp.concatenate([mix_in[half, n, here, :] for n in range(4)], axis=1).astype(F32)
+            data = (resid[rows, :].astype(F32) + mixed).astype(BF)
+            mid[rows, :] = data
+            v = data.astype(F32)
+            scale = lax.rsqrt(jnp.mean(v * v, axis=-1, keepdims=True) + 1e-06)
+            at = pl.multiple_of(tp * RB + half * 96 + i * 16, 16)
+            x2[pl.ds(at, 16), :] = (v * scale * gain2[...]).astype(BF)
             return carry
 
         cp.arrived(mix_in.at[half], mix_sem + half)
-        lax.fori_loop(0, 4, step, 0)
-        norm_rows(mid, gain2, x2, tp * RB, 6 * half, 6)
+        lax.fori_loop(0, 6, step, 0)
 
     steps["c.p0"], steps["c.p1"] = (lambda: point(0)), (lambda: point(1))
     steps["c.m0"], steps["c.m1"] = (lambda: middle(0)), (lambda: middle(1))
@@ -539,14 +577,20 @@
     steps["c.um"] = lambda: up(xm)
     steps["c.uf"] = lambda: up(xf)
 
-    pair_sem = {"f": cp.take(8), "pl": cp.take(4), "la": cp.take(4), "x": cp.take()}
+    pair_sem = {"f": cp.take(8), "pl": cp.take(8), "la": cp.take(4), "x": cp.take()}
     relay_sem, end_sem = cp.take(4), cp.take(4)
     pair_send, ring_send = cp.take_send(par_out), cp.take_send(par.at[0:3])
 
-    def place(i):
-        dz = (i % 4 + 3 * (i // 4)) % 4
-        turn = (dz // 2 + i // 4) % 2
-        return ((z + dz) % 4) * 2 + (y // 2 + turn) % 2
+    def blocks(i):
+        return [((z + dz) % 4, (y + dy) % 4) for dz, dy in CHUNKS[i]]
+
+    def block_columns(owner):
+        return pl.ds(pl.multiple_of((owner[0] * 4 + owner[1]) * 128, 128), 128)
+
+    def down_columns(i):
+        (za, ya), (zb, yb) = blocks(i)
+        halves = [jnp.concatenate([dd[half, za, ya], dd[half, zb, yb]], axis=1) for half in range(2)]
+        return jnp.concatenate(halves, axis=0)
 
     def down(*chunks):
         done = []
@@ -554,7 +598,7 @@
             pair_rows = pl.ds(pl.multiple_of(v * CB + (1 - c) * RB, RB), RB)
             own_rows = pl.ds(pl.multiple_of(v * CB + c * RB, RB), RB)
             rows = jnp.concatenate([hid[pair_rows, :], hid[own_rows, :]], axis=0)
-            done.append(dot(rows, columns(dd, place(i))))
+            done.append(dot(rows, down_columns(i)))
         for (v, i, _), both in zip(chunks, done):
             par_out[v, i] = both[:RB].astype(BF)
             par[v, i] = both[RB:].astype(BF)
@@ -582,11 +626,8 @@
         cp.copy(par.at[to, n], fin_in.at[side, n], peer, end_sem + k, ring_send).start()
 
     def each(count, body):
-        def step(i, carry):
+        for i in range(count):
             body(i)
-            return carry
-
-        lax.fori_loop(0, count, step, 0)
 
     def relay_chunk(side, k):
         n = side * 4 + k
@@ -594,57 +635,54 @@
         add_pair(xf, n)
         relay(side, k)
 
-    def plain_chunk(k):
-        pair_arrived(pair_sem["pl"] + k, 2)
-        add_pair(xp, k + 4)
-        plain(0, k)
-        add_pair(xm, k)
-        plain(1, k)
-
-    def far_two(k):
-        down((xf, k, pair_sem["f"] + k), (xf, k + 4, pair_sem["f"] + k + 4))
-
-    def near_two(k):
-        down((xp, k + 4, pair_sem["pl"] + k), (xm, k, pair_sem["pl"] + k))
-
-    steps["d.ep"] = lambda: near_two(0)
+    def plain_chunk(side, k):
+        pair_arrived(pair_sem["pl"] + 4 * side + k, 1)
+        add_pair(xm if side else xp, k if side else k + 4)
+        plain(side, k)
+
+    def far(i):
+        return xf, i, pair_sem["f"] + i
+
+    def near(side, k):
+        return xm if side else xp, k if side else k + 4, pair_sem["pl"] + 4 * side + k
+
+    @step_named("d.ep")
+    def _():
+        down(near(0, 0), near(1, 0))
+        down(near(0, 1), near(1, 1))
 
     @step_named("d.ef")
     def _():
-        far_two(0)
-        down((xf, 1, pair_sem["f"] + 1))
-
-    steps["d.sp"] = lambda: plain_chunk(0)
+        down(far(0), far(4))
+        down(far(1), far(5))
+
+    @step_named("d.sp")
+    def _():
+        for k in range(2):
+            for side in range(2):
+                plain_chunk(side, k)
 
     @step_named("d.sf")
     def _():
-        relay_chunk(0, 0)
-        relay_chunk(1, 0)
-        relay_chunk(0, 1)
+        for k in range(2):
+            for side in range(2):
+                relay_chunk(side, k)
 
     @step_named("d.fa")
     def _():
-        down((xf, 5, pair_sem["f"] + 5), (xf, 2, pair_sem["f"] + 2))
-
-        down((xf, 6, pair_sem["f"] + 6), (xf, 3, pair_sem["f"] + 3))
-        relay_chunk(1, 1)
-        relay_chunk(0, 2)
-        down((xf, 7, pair_sem["f"] + 7))
-        relay_chunk(1, 2)
-        relay_chunk(0, 3)
-        relay_chunk(1, 3)
+        down(far(2), far(6))
+        down(far(3), far(7))
+        for k in range(2, 4):
+            for side in range(2):
+                relay_chunk(side, k)
 
     @step_named("d.pl")
     def _():
-        def near_step(k):
-            near_two(k)
-
-            @pl.when(k >= 2)
-            def _():
-                plain_chunk(k - 1)
-
-        each(3, lambda k: near_step(k + 1))
-        plain_chunk(3)
+        down(near(0, 2), near(1, 2))
+        down(near(0, 3), near(1, 3))
+        for k in range(2, 4):
+            for side in range(2):
+                plain_chunk(side, k)
 
     @step_named("d.la")
     def _():
@@ -668,23 +706,22 @@
         each(4, lambda k: down((x, k, pair_sem["x"]), (x, k + 4, pair_sem["x"])))
         pair_arrived(pair_sem["x"], 8)
 
-        def own_step(n):
-            cols = pl.ds(pl.multiple_of(place(n) * 256, 256), 256)
-            mix[:, cols] = mid[:, cols].astype(F32) + (par[x, n].astype(F32) + par_in[x, n].astype(F32))
+        def own_step(i):
+            for part, owner in enumerate(blocks(i)):
+                lane, cols = slice(part * 128, part * 128 + 128), block_columns(owner)
+                own = par[x, i, :, lane].astype(F32) + par_in[x, i, :, lane].astype(F32)
+                mix[:, cols] = mid[:, cols].astype(F32) + own
 
         each(8, own_step)
-
-    def out_copy(n):
-        cols = pl.ds(pl.multiple_of(place(n) * 256, 256), 256)
-        return pltpu.make_async_copy(out_buf.at[n], out.at[:, cols], out_sem.at[0])
 
     def finish(k):
         cp.arrived(fin_in.at[0, 0:4], end_sem + k)
-        for n in (k, k + 4):
-            cols = pl.ds(pl.multiple_of(place(n) * 256, 256), 256)
-            total = fin_in[0, n].astype(F32) + fin_in[1, n].astype(F32)
-            out_buf[n] = (mix[:, cols] + total).astype(BF)
-            out_copy(n).start()
+        for i in (k, k + 4):
+            total = fin_in[0, i].astype(F32) + fin_in[1, i].astype(F32)
+            for part, owner in enumerate(blocks(i)):
+                lane, cols = slice(part * 128, part * 128 + 128), block_columns(owner)
+                out_buf[i, part] = (mix[:, cols] + total[:, lane]).astype(BF)
+                pltpu.make_async_copy(out_buf.at[i, part], out.at[:, cols], out_sem.at[0]).start()
 
     steps["d.fn"] = lambda: each(4, finish)
     pl.semaphore_wait(barrier, 7)
@@ -706,8 +743,8 @@
     ((SEQ + 2 * HALO, CW), BF),
     ((4, CB + 2 * HALO, CW), BF),
     ((4, CB, CW), F32),
-    ((2, CB, 128), F32),
-    ((2, CB, 128), F32),
+    ((2, 2, RB, 128), F32),
+    ((2, 2, RB, 128), F32),
     ((CB, 4 * CW), BF),
     ((2, 4, 96, 512), BF),
     ((2, 4, 96, 512), BF),
@@ -720,7 +757,7 @@
     ((2, 4, RB, 256), BF),
     ((2, 8, RB, 256), BF),
     ((2, FAR, CW), BF),
-    ((8, RB, 256), BF),
+    ((8, 2, RB, 128), BF),
 )
 
 

time: 116 us -> 113 us (0.974)
  Pallas kernels: 113 us -> 111 us
    pallas_call x1, Pallas kernels: 113 us -> 111 us  [shards(): pl.pallas_call(kernel, out_shape=jax.ShapeDtypeStruct((RB, D), BF), in_sp...]
where the time goes in v5:
time: 113 us
  Pallas kernels  111 us (98%)
  local copies, waits for them, and re-layouts  2.09 us (2%)
    pallas_call x1, Pallas kernels, shards(): pl.pallas_call(kernel, out_shape=jax.ShapeDtypeStruct((RB, D), BF), in_sp...  111 us

profile of v5, /device:TPU:1, one launch (start us, length us, event | category | flops | bytes accessed | tf_op | source)
XLA Modules:
  0.0 113.3 jit_solution(3420824408564725560)
XLA Ops:
  0.0 111.2 %layer.1 = bf16[192,2048]{1,0:T(8,128)(2,1)} custom-call(bf16[192,2048]{1,0:T(8,128)(2,1)} %refs_0_.1, f32[1,2048]{1,0:T(1,128)} %bitcast.8, f32[128,256]{1,0:T(8,128)} %refs_2_.1, f32[128,256]{1,0:T(8,128)} %refs_3_.1, f32[1,2048]{1,0:T(1,128)} %bitcast.9, f32[1,2048]{1,0:T(1,128)} %bitcast.10, f32[31,2048]{1,0:T(8,128)} %refs_6_.1, f32[1,2048]{1,0:T(1,128)} %bitcast.11, ...), custom_call_target="tpu_custom_call" | custom-call | tf_op jit(solution)/shard_map/layer/pallas_call | solution.py:766
  111.2 2.1 %copy.17 = bf16[192,2048]{1,0:T(8,128)(2,1)} copy(bf16[192,2048]{1,0:T(8,128)(2,1)} %layer.1) | data formatting | bytes 1572864

commit v6 on v5

--- a/solution.py
+++ b/solution.py
@@ -24,13 +24,13 @@
 N_SEND, N_RECV = 12, 96
 
 ORDER = (
-    "c.ld", "V.s0", "px.0", "U.s0", "c.n1", "R1.oa", "px.1", "V.s1", "D.s0", "R1.ob", "V.s2", "px.2", "P.s0",
-    "c.init", "U.s1", "R1.oc", "R1.ra", "R1.rb", "P.s1", "V.s3", "R1.nr", "P.s2", "R1.nw", "R1.fa", "V.s4",
-    "c.gx", "c.gp", "c.sp", "c.gm", "R1.fb", "c.g0", "R1.fw", "c.gf", "c.cx", "P.s3", "D.s1", "c.f0", "c.f1",
+    "c.ld", "V.s0", "px.0", "U.s0", "D.s0", "c.n1", "R1.oa", "px.1", "V.s1", "U.s1", "R1.ob", "R1.oc", "D.s1",
+    "px.2", "P.s0", "V.s2", "c.init", "R1.ra", "R1.rb", "P.s1", "V.s3", "R1.nr", "P.s2", "R1.nw", "V.s4",
+    "c.gx", "c.gp", "c.sp", "R1.fa", "c.gm", "R1.fb", "c.g0", "R1.fw", "c.gf", "c.cx", "P.s3", "c.f0", "c.f1",
     "c.f2", "c.cm", "U.s2", "c.cp", "c.cf", "c.a0", "P.s4", "c.p0", "c.a1", "c.m0", "R2.oa", "c.p1", "U.s3",
-    "c.m1", "D.s2", "R2.ob", "R2.ra", "U.s4", "c.ux", "R2.rb", "D.s3", "R2.nr", "R2.nw", "c.up", "c.um",
-    "R2.fa", "D.s4", "d.ep", "d.sp", "R2.fb", "R2.fw", "c.uf", "d.ef", "d.sf", "D.s5", "d.pl", "d.fa", "d.la",
-    "d.sl", "d.xx", "d.fn",
+    "c.m1", "D.s2", "R2.ob", "R2.ra", "U.s4", "c.ux", "R2.rb", "R2.nr", "D.s3", "R2.nw", "c.up", "c.um",
+    "R2.fa", "D.s4", "d.e0", "d.e1", "d.s0", "d.s1", "R2.fb", "c.u0", "R2.fw", "c.uf", "d.ef", "d.sf", "D.s5",
+    "d.pl", "d.fa", "d.la", "d.sl", "d.xx", "d.fn",
 )
 
 
@@ -535,7 +535,8 @@
             mix[half * 96 : half * 96 + 96, pl.ds(pl.multiple_of(n * 512, 512), 512)] = both[96:]
             return carry
 
-        lax.fori_loop(0, 4, step, 0)
+        for n in range(4):
+            step(n, 0)
 
     def middle(half):
         def step(i, carry):
@@ -557,7 +558,10 @@
     steps["c.m0"], steps["c.m1"] = (lambda: middle(0)), (lambda: middle(1))
 
     def up(v):
-        rows = pl.ds(pl.multiple_of(v * CB, CB), CB)
+        up_rows(v * CB, CB)
+
+    def up_rows(first, count):
+        rows = pl.ds(pl.multiple_of(first, 64), count)
 
         def step(n, carry):
             weight = uu[n].reshape(D, 512)
@@ -566,7 +570,8 @@
             hid[rows, cols] = (upper * upper).astype(BF)
             return carry
 
-        lax.fori_loop(0, 2, step, 0)
+        for n in range(2):
+            step(n, 0)
 
     @step_named("c.ux")
     def _():
@@ -575,7 +580,8 @@
 
     steps["c.up"] = lambda: up(xp)
     steps["c.um"] = lambda: up(xm)
-    steps["c.uf"] = lambda: up(xf)
+    steps["c.u0"] = lambda: up_rows(xf * CB + c * RB, RB)
+    steps["c.uf"] = lambda: up_rows(xf * CB + (1 - c) * RB, RB)
 
     pair_sem = {"f": cp.take(8), "pl": cp.take(8), "la": cp.take(4), "x": cp.take()}
     relay_sem, end_sem = cp.take(4), cp.take(4)
@@ -646,21 +652,20 @@
     def near(side, k):
         return xm if side else xp, k if side else k + 4, pair_sem["pl"] + 4 * side + k
 
-    @step_named("d.ep")
-    def _():
-        down(near(0, 0), near(1, 0))
-        down(near(0, 1), near(1, 1))
+    for side in range(2):
+        steps[f"d.e{side}"] = lambda side=side: down(near(side, 0), near(side, 1))
 
     @step_named("d.ef")
     def _():
         down(far(0), far(4))
         down(far(1), far(5))
 
-    @step_named("d.sp")
-    def _():
-        for k in range(2):
-            for side in range(2):
-                plain_chunk(side, k)
+    def send_plain(side):
+        plain_chunk(side, 0)
+        plain_chunk(side, 1)
+
+    for side in range(2):
+        steps[f"d.s{side}"] = lambda side=side: send_plain(side)
 
     @step_named("d.sf")
     def _():

time: 113 us -> 112 us (level)
    pallas_call x1, Pallas kernels: 111 us -> 110 us  [shards(): pl.pallas_call(kernel, out_shape=jax.ShapeDtypeStruct((RB, D), BF), in_sp...]
where the time goes in v6:
time: 112 us
  Pallas kernels  110 us (98%)
  local copies, waits for them, and re-layouts  2.09 us (2%)
    pallas_call x1, Pallas kernels, shards(): pl.pallas_call(kernel, out_shape=jax.ShapeDtypeStruct((RB, D), BF), in_sp...  110 us

profile of v6, /device:TPU:1, one launch (start us, length us, event | category | flops | bytes accessed | tf_op | source)
XLA Modules:
  0.0 112.0 jit_solution(10291247844726167379)
XLA Ops:
  0.0 109.9 %layer.1 = bf16[192,2048]{1,0:T(8,128)(2,1)} custom-call(bf16[192,2048]{1,0:T(8,128)(2,1)} %refs_0_.1, f32[1,2048]{1,0:T(1,128)} %bitcast.8, f32[128,256]{1,0:T(8,128)} %refs_2_.1, f32[128,256]{1,0:T(8,128)} %refs_3_.1, f32[1,2048]{1,0:T(1,128)} %bitcast.9, f32[1,2048]{1,0:T(1,128)} %bitcast.10, f32[31,2048]{1,0:T(8,128)} %refs_6_.1, f32[1,2048]{1,0:T(1,128)} %bitcast.11, ...), custom_call_target="tpu_custom_call" | custom-call | tf_op jit(solution)/shard_map/layer/pallas_call | solution.py:771
  109.9 2.1 %copy.17 = bf16[192,2048]{1,0:T(8,128)(2,1)} copy(bf16[192,2048]{1,0:T(8,128)(2,1)} %layer.1) | data formatting | bytes 1572864

commit v7 on v6

--- a/solution.py
+++ b/solution.py
@@ -21,10 +21,10 @@
 FAR = 208
 KERNEL = 31
 GROUP_WIDTH = 512.0
-N_SEND, N_RECV = 12, 96
+N_SEND, N_RECV = 12, 77
 
 ORDER = (
-    "c.ld", "V.s0", "px.0", "U.s0", "D.s0", "c.n1", "R1.oa", "px.1", "V.s1", "U.s1", "R1.ob", "R1.oc", "D.s1",
+    "c.ld", "V.s0", "px.0", "U.s0", "D.s0", "c.n1", "R1.oa", "px.1", "R1.ob", "R1.oc", "V.s1", "U.s1", "D.s1",
     "px.2", "P.s0", "V.s2", "c.init", "R1.ra", "R1.rb", "P.s1", "V.s3", "R1.nr", "P.s2", "R1.nw", "V.s4",
     "c.gx", "c.gp", "c.sp", "R1.fa", "c.gm", "R1.fb", "c.g0", "R1.fw", "c.gf", "c.cx", "P.s3", "c.f0", "c.f1",
     "c.f2", "c.cm", "U.s2", "c.cp", "c.cf", "c.a0", "P.s4", "c.p0", "c.a1", "c.m0", "R2.oa", "c.p1", "U.s3",
@@ -235,9 +235,9 @@
             self.share("far", (xf, 3, 1))
 
     class Weights:
-        def __init__(self, buf):
-            self.buf, self.deep = buf, buf.shape[3]
-            self.sem = [cp.take() for _ in range(6)]
+        def __init__(self, buf, apart=0):
+            self.buf, self.deep, self.apart = buf, buf.shape[3], apart
+            self.sem = [cp.take() for _ in range(4 + apart)]
             rows = 30 * buf.shape[3] * buf.shape[4] // D
             self.send = cp.take_send(x1.at[0:rows])
 
@@ -268,11 +268,10 @@
                 (self.buf.at[1, zp, y, hi], to_zm),
             )
             cp.arrived(self.buf.at[0, 0, 0:2], self.sem[0])
-            self.four(2, plan)
+            self.four(1, plan)
 
         def s2(self):
-            cp.arrived(self.buf.at[0, 0, 0:2], self.sem[1])
-            cp.arrived(self.buf.at[0, 0, 0:2], self.sem[2])
+            cp.arrived(self.buf.at[0, 0], self.sem[1])
             parts = pl.ds(0, 2), pl.ds(2, 2)
             for turn in range(2):
                 lo, hi = parts[turn], parts[1 - turn]
@@ -282,7 +281,7 @@
                     (self.buf.at[0, z, hi], to_zm),
                     (self.buf.at[1, hi, y], to_ym),
                 )
-                self.four(3 + turn, plan)
+                self.four(2 + turn, plan)
 
         def s3(self):
             lo, hi = pl.ds(0, 2), pl.ds(2, 2)
@@ -292,15 +291,14 @@
                 (self.buf.at[0, zp, hi], to_zm),
                 (self.buf.at[1, hi, yp], to_ym),
             )
-            cp.arrived(self.buf.at[0, 0:2], self.sem[3])
-            self.four(5, plan)
+            cp.arrived(self.buf.at[0, 0:2], self.sem[2])
+            self.four(3 + self.apart, plan)
 
         def s4(self):
-            cp.arrived(self.buf.at[0, 0:2], self.sem[4])
-            cp.arrived(self.buf.at[0, 0:2], self.sem[5])
+            cp.arrived(self.buf.at[0], self.sem[3])
 
     ring1, ring2 = Ring(x1), LateRing(x2)
-    gv, gp, gu, gd = Weights(vg), Weights(pp), Weights(uu), Weights(dd)
+    gv, gp, gu, gd = Weights(vg), Weights(pp), Weights(uu), Weights(dd, 1)
 
     steps = {}
 
@@ -314,8 +312,8 @@
     for name, chain in (("V", gv), ("P", gp), ("U", gu), ("D", gd)):
         for part in ("s0", "s1", "s2", "s3", "s4"):
             steps[name + "." + part] = getattr(chain, part)
-    steps["D.s4"] = lambda: cp.arrived(dd.at[0, 0:2], gd.sem[4])
-    steps["D.s5"] = lambda: cp.arrived(dd.at[0, 0:2], gd.sem[5])
+    steps["D.s4"] = lambda: cp.arrived(dd.at[0, 0:2], gd.sem[3])
+    steps["D.s5"] = lambda: cp.arrived(dd.at[0, 0:2], gd.sem[4])
     steps["R1.oc"] = ring1.oc
     for name, chain in (("R1", ring1), ("R2", ring2)):
         for part in ("oa", "ob", "ra", "rb", "nr", "nw", "fa", "fb", "fw"):

time: 112 us -> 112 us (level)
  no operation moved by 1% of the time
where the time goes in v7:
time: 112 us
  Pallas kernels  110 us (98%)
  local copies, waits for them, and re-layouts  2.09 us (2%)
    pallas_call x1, Pallas kernels, shards(): pl.pallas_call(kernel, out_shape=jax.ShapeDtypeStruct((RB, D), BF), in_sp...  110 us

profile of v7, /device:TPU:1, one launch (start us, length us, event | category | flops | bytes accessed | tf_op | source)
XLA Modules:
  0.0 112.2 jit_solution(5585061778563607601)
XLA Ops:
  0.0 110.1 %layer.1 = bf16[192,2048]{1,0:T(8,128)(2,1)} custom-call(bf16[192,2048]{1,0:T(8,128)(2,1)} %refs_0_.1, f32[1,2048]{1,0:T(1,128)} %bitcast.8, f32[128,256]{1,0:T(8,128)} %refs_2_.1, f32[128,256]{1,0:T(8,128)} %refs_3_.1, f32[1,2048]{1,0:T(1,128)} %bitcast.9, f32[1,2048]{1,0:T(1,128)} %bitcast.10, f32[31,2048]{1,0:T(8,128)} %refs_6_.1, f32[1,2048]{1,0:T(1,128)} %bitcast.11, ...), custom_call_target="tpu_custom_call" | custom-call | tf_op jit(solution)/shard_map/layer/pallas_call | solution.py:769
  110.1 2.1 %copy.17 = bf16[192,2048]{1,0:T(8,128)(2,1)} copy(bf16[192,2048]{1,0:T(8,128)(2,1)} %layer.1) | data formatting | bytes 1572864
